TPU v7x, 256 devices: a whole 4x4x8 slice. The times are simulated.
256 devices in a mesh: ep: 64 (over z, x, core), tp: 4 (over y).
Axes of the slice: x: 4, y: 4, z: 8, core: 2. Of those that a mesh axis runs over, the one named last changes fastest.
Arguments:
- conv_input: bfloat16 [65536, 2048], P('ep', 'tp'), may hold values from -6 to 6
- conv_kernel: bfloat16 [31, 2048], P(None, 'tp'), may hold values from -2 to 2
- norm_gain: float32 [2048], P('tp'), may hold values from 0.1 to 1.9
- norm_shift: float32 [2048], P('tp'), may hold values from -3 to 3
- conv_proj: bfloat16 [2048, 2048], P('tp'), may hold values from -0.125 to 0.125
- moe_input: bfloat16 [16384, 2048], P(('ep', 'tp')), may hold values from -6 to 6
- moe_gain: float32 [2048], replicated, may hold values from 0.1 to 1.9
- routes: int32 [16384, 2], P('ep'), may hold values from 0 to 63, all different within a row; in each aligned block of 256 rows (0 to 255, 256 to 511, ...) at most 16 rows name the same one
- route_weights: float32 [16384, 2], P('ep'), may hold values from 0.2 to 1
- gate_proj: bfloat16 [64, 2048, 2048], P('ep', None, 'tp'), may hold values from -0.125 to 0.125
- up_proj: bfloat16 [64, 2048, 2048], P('ep', None, 'tp'), may hold values from -0.125 to 0.125
- down_proj: bfloat16 [64, 2048, 2048], P('ep', 'tp'), may hold values from -0.125 to 0.125
Outputs:
- conv_out: bfloat16 [65536, 2048], P(('ep', 'tp'))
- moe_out: bfloat16 [16384, 2048], P(('ep', 'tp'))
Inputs may be any that keep to these rules, and one draw needn't show every extreme that they name: `routes`: each row names 2 different experts. In each aligned block of 256 rows no expert is named by more than 16 rows, and in some blocks an expert is named by exactly 16 rows.
All inputs are finite; a program needn't handle non-finite values.
Results may differ from a plain program's by a relative error of at most 0.012.
Values may be sent and summed in bfloat16 or wider, within the bound.
A program may use at most 128 MiB of HBM per device.

v0:
```python
import functools

import jax
import jax.numpy as jnp
from jax import lax
from jax.experimental import pallas as pl
from jax.experimental.pallas import tpu as pltpu
from jax.sharding import PartitionSpec as P

MESH = pl.DeviceIdType.MESH


def hop_order(ep_count):
    half = ep_count // 2
    order = [0, half]
    for near in range(1, half):
        order += [half - near, half + near]
    return order


def exchange(
    normed, ranks, weights, mixed, stats, gain, shift, proj, gate_hbm, up_hbm, down_hbm,
    conv_out, moe_out,
    partial, stats_in, columns, gate, up, down, group, outgoing, arrived, pieces, from_core, to_y, from_y, to_ep, returned,
    conv_core, conv_to_y, conv_from_y, combined, last_core, last_to_y, last_from_y,
    weight_sem, stats_send, stats_recv, ag_send, ag_recv, ep_send, ep_recv, fan_send, fan_recv,
    core_send, core_recv, y_send, y_recv, back_send, back_recv,
    conv_send, conv_recv, last_send, last_recv,
    *, ep_count, share,
):
    order = hop_order(ep_count)
    me_ep, me = lax.axis_index("ep"), lax.axis_index("tp")
    core = me + 1 - 2 * (me % 2)
    over = (me + 2) % 4
    far = (core + 2) % 4
    rows, width = normed.shape
    f32, bf16 = jnp.float32, jnp.bfloat16

    def remote(src, dst, send, recv, where):
        return pltpu.make_async_remote_copy(
            src_ref=src, dst_ref=dst, send_sem=send, recv_sem=recv, device_id=where,
            device_id_type=MESH,
        )

    def block(ref, index, size):
        return ref.at[pl.ds(pl.multiple_of(index * size, size), size)]

    loads = [
        pltpu.make_async_copy(src, dst, weight_sem.at[i])
        for i, (src, dst) in enumerate(((gate_hbm, gate), (up_hbm, up), (down_hbm, down)))
    ]
    for load in loads:
        load.start()
    barrier = pltpu.get_barrier_semaphore()
    pl.semaphore_signal(barrier, inc=1, device_id={"tp": core}, device_id_type=MESH)
    pl.semaphore_signal(barrier, inc=1, device_id={"tp": over}, device_id_type=MESH)
    pl.semaphore_signal(barrier, inc=1, device_id={"tp": far}, device_id_type=MESH)
    for d in range(1, ep_count):
        pl.semaphore_signal(
            barrier, inc=1, device_id={"ep": (me_ep + d) % ep_count}, device_id_type=MESH
        )
    pl.semaphore_wait(barrier, ep_count + 2)

    sent = []

    ag = [
        remote(normed, block(group, me, rows), ag_send.at[0], ag_recv.at[0], {"tp": over}),
        remote(normed, block(group, me, rows), ag_send.at[1], ag_recv.at[1], {"tp": core}),
        remote(block(group, over, rows), block(group, over, rows), ag_send.at[2], ag_recv.at[2], {"tp": core}),
    ]
    moments = [
        remote(stats, stats_in.at[n], stats_send.at[n], stats_recv.at[n], {"tp": where})
        for n, where in enumerate((over, core, far))
    ]
    sent += moments
    ag[0].start()
    ag[1].start()
    for r in moments:
        r.start()
    group[pl.ds(pl.multiple_of(me * rows, rows), rows), :] = normed[...]
    span = partial.shape[0] // 4
    conv = [
        remote(
            block(partial, core if n == 0 else far, span), conv_core.at[n],
            conv_send.at[n], conv_recv.at[n], {"tp": core},
        )
        for n in range(2)
    ]
    ag[0].wait_recv()
    ag[2].start()
    ag[1].wait_recv()
    ag[2].wait_recv()
    sent += ag + conv

    tile = 512
    group_rows = ranks.shape[1]
    wanted = me * share + lax.broadcasted_iota(jnp.int32, (share, group_rows), 0)
    held = [ranks[s : s + 1, :] == wanted for s in range(ep_count)]
    pick = jnp.concatenate([jnp.where(h, 1.0, 0.0) for h in held], axis=0).astype(bf16)
    for n in range(0, width, tile):
        part = jnp.dot(pick, group[:, n : n + tile], preferred_element_type=f32).astype(bf16)
        outgoing[:, n : n + tile] = part
        arrived[pl.ds(pl.multiple_of(me * share, share), share), n : n + tile] = part[:share]
    ep = []
    for s in range(1, ep_count):
        ep.append(
            remote(
                outgoing.at[s * share : (s + 1) * share], block(arrived, s * 4 + me, share),
                ep_send.at[s], ep_recv.at[s], {"ep": (me_ep + order[s]) % ep_count},
            )
        )
        ep[-1].start()
    sent += ep

    def center_and_scale():
        for r in moments:
            r.wait_recv()
        total = (stats[...] + stats_in[0] + stats_in[1] + stats_in[2]) / width
        center = total[0:1, :]
        spread = jnp.maximum(total[1:2, :] - center * center, 0.0)
        both = jnp.concatenate([center, lax.rsqrt(spread + 1e-05)] + [center] * 6, axis=0)
        columns[...] = both.T

    def project(quarter):
        at = pl.multiple_of(quarter * span, span)
        view = pl.ds(at, span)
        col = columns[view, :]
        scaled = (mixed[view, :] - col[:, 0:1]) * col[:, 1:2] * gain[...] + shift[...]
        activated = (scaled / (1.0 + jnp.exp(-scaled))).astype(bf16)
        for n in range(0, width, tile):
            partial[view, n : n + tile] = jnp.dot(
                activated, proj[:, n : n + tile], preferred_element_type=f32
            ).astype(bf16)

    def fan(kind, s):
        quarter = over if kind == 2 else me
        place = block(arrived, s * 4 + quarter, share)
        return remote(
            place, place, fan_send.at[kind, s], fan_recv.at[kind, s],
            {"tp": over if kind == 0 else core},
        )

    fans = [[fan(kind, s) for s in range(ep_count)] for kind in range(3)]
    for kind in range(3):
        sent += fans[kind]

    def relay(s):
        fans[0][s].wait_recv()
        fans[2][s].start()

    def land(s):
        if s > 0:
            ep[s - 1].wait_recv()
        fans[0][s].start()
        fans[1][s].start()

    conv_y = [
        remote(conv_to_y.at[n], conv_from_y.at[n], conv_send.at[2 + n], conv_recv.at[2 + n], {"tp": over})
        for n in range(4)
    ]
    sent += conv_y
    piece_rows = span // 4

    def conv_half():
        conv[1].wait_recv()
        for n in range(4):
            at = pl.multiple_of(over * span + n * piece_rows, piece_rows)
            conv_to_y[n] = (
                partial[pl.ds(at, piece_rows), :].astype(f32)
                + conv_core[1, n * piece_rows : (n + 1) * piece_rows, :].astype(f32)
            ).astype(bf16)
            conv_y[n].start()

    chunk = 2 * 4 * share

    def experts(c):
        for s in (2 * c, 2 * c + 1):
            fans[1][s].wait_recv()
            fans[2][s].wait_recv()
        here = slice(c * chunk, (c + 1) * chunk)
        lines = arrived[here, :]
        left = jnp.dot(lines, gate[...], preferred_element_type=f32)
        right = jnp.dot(lines, up[...], preferred_element_type=f32)
        hidden = (left / (1.0 + jnp.exp(-left)) * right).astype(bf16)
        for n in range(0, width, tile):
            pieces[here, n : n + tile] = jnp.dot(
                hidden, down[:, n : n + tile], preferred_element_type=f32
            ).astype(bf16)
        for s in (2 * c, 2 * c + 1):
            cores[s][1].start()
            cores[s][0].start()

    cores = [
        [
            remote(
                block(pieces, s * 4 + (core if n == 0 else far), share), from_core.at[s, n],
                core_send.at[s, n], core_recv.at[s, n], {"tp": core},
            )
            for n in range(2)
        ]
        for s in range(ep_count)
    ]
    ys = [
        remote(to_y.at[s], from_y.at[s], y_send.at[s], y_recv.at[s], {"tp": over})
        for s in range(ep_count)
    ]
    backs = [
        remote(
            to_ep.at[s], returned.at[s * share : (s + 1) * share], back_send.at[s], back_recv.at[s],
            {"ep": (me_ep + ep_count - order[s]) % ep_count},
        )
        for s in range(1, ep_count)
    ]
    for s in range(ep_count):
        sent += cores[s]
    sent += ys + backs

    def mine(s, quarter, n):
        at = pl.multiple_of((s * 4 + quarter) * share, share)
        return pieces[pl.ds(at, share), :].astype(f32) + from_core[s, n].astype(f32)

    def across(c):
        for s in (2 * c, 2 * c + 1):
            cores[s][1].wait_recv()
            to_y[s] = mine(s, over, 1).astype(bf16)
            ys[s].start()

    def back(c):
        for s in (2 * c, 2 * c + 1):
            cores[s][0].wait_recv()
            ys[s].wait_recv()
            total = (mine(s, me, 0) + from_y[s].astype(f32)).astype(bf16)
            if s == 0:
                returned[:share, :] = total
            else:
                to_ep[s] = total
                backs[s - 1].start()

    chunks = ep_count // 2
    land(0)
    for s in range(1, ep_count):
        land(s)
        if s >= 2:
            relay(s - 2)
        if s == 1:
            center_and_scale()
            project(far)
            conv[1].start()
        if s == 2:
            project(core)
            conv[0].start()
        if s == 3:
            project(over)
        if s == 4:
            project(me)
        if s == 3:
            for load in loads:
                load.wait()
        if s == 5:
            experts(0)
    experts(1)
    across(0)
    relay(ep_count - 2)
    relay(ep_count - 1)
    conv_half()
    for c in range(2, chunks):
        experts(c)
        across(c - 1)
        back(c - 2)
    across(chunks - 1)
    back(chunks - 2)
    conv[0].wait_recv()
    for n in range(4):
        conv_y[n].wait_recv()
        at = pl.multiple_of(me * span + n * piece_rows, piece_rows)
        conv_out[n * piece_rows : (n + 1) * piece_rows, :] = (
            partial[pl.ds(at, piece_rows), :].astype(f32)
            + conv_core[0, n * piece_rows : (n + 1) * piece_rows, :].astype(f32)
            + conv_from_y[n].astype(f32)
        ).astype(bf16)
    back(chunks - 1)

    for r in backs:
        r.wait_recv()
    scale = jnp.concatenate(
        [jnp.where(h, weights[s : s + 1, :], 0.0) for s, h in enumerate(held)], axis=0
    ).T.astype(bf16)
    for n in range(0, width, tile):
        combined[:, n : n + tile] = jnp.dot(
            scale, returned[:, n : n + tile], preferred_element_type=f32
        ).astype(bf16)
    last = [
        remote(
            block(combined, core if n == 0 else far, rows), last_core.at[n],
            last_send.at[n], last_recv.at[n], {"tp": core},
        )
        for n in range(2)
    ]
    last[1].start()
    last[0].start()
    last.append(remote(last_to_y, last_from_y, last_send.at[2], last_recv.at[2], {"tp": over}))

    def own(quarter, n):
        at = pl.multiple_of(quarter * rows, rows)
        return combined[pl.ds(at, rows), :].astype(f32) + last_core[n].astype(f32)

    last[1].wait_recv()
    last_to_y[...] = own(over, 1).astype(bf16)
    last[2].start()
    last[0].wait_recv()
    last[2].wait_recv()
    moe_out[...] = (own(me, 0) + last_from_y[...].astype(f32)).astype(bf16)
    sent += last
    for r in sent:
        r.wait_send()


def run_exchange(
    normed, ranks, weights, mixed, stats, gain, shift, proj, gate, up, down, ep_count, share
):
    rows, width = normed.shape
    hid = gate.shape[1]
    conv_rows = mixed.shape[0]
    span = conv_rows // 4
    bf16 = jnp.bfloat16
    slots = ep_count * share
    vmem, dma = pltpu.VMEM, pltpu.SemaphoreType.DMA
    at_vmem, at_any = pl.BlockSpec(memory_space=pltpu.VMEM), pl.BlockSpec(memory_space=pl.ANY)
    return pl.pallas_call(
        functools.partial(exchange, ep_count=ep_count, share=share),
        out_shape=(
            jax.ShapeDtypeStruct((span, width), bf16),
            jax.ShapeDtypeStruct((rows, width), bf16),
        ),
        in_specs=[at_vmem] * 8 + [at_any] * 3,
        out_specs=(at_vmem, at_vmem),
        scratch_shapes=[
            vmem((conv_rows, width), bf16),
            vmem((3, 8, conv_rows), jnp.float32),
            vmem((conv_rows, 8), jnp.float32),
            vmem((width, hid), bf16),
            vmem((width, hid), bf16),
            vmem((hid, width), bf16),
            vmem((4 * rows, width), bf16),
            vmem((slots, width), bf16),
            vmem((4 * slots, width), bf16),
            vmem((4 * slots, width), bf16),
            vmem((ep_count, 2, share, width), bf16),
            vmem((ep_count, share, width), bf16),
            vmem((ep_count, share, width), bf16),
            vmem((ep_count, share, width), bf16),
            vmem((slots, width), bf16),
            vmem((2, span, width), bf16),
            vmem((4, span // 4, width), bf16),
            vmem((4, span // 4, width), bf16),
            vmem((4 * rows, width), bf16),
            vmem((2, rows, width), bf16),
            vmem((rows, width), bf16),
            vmem((rows, width), bf16),
            dma((3,)),
            dma((3,)), dma((3,)),
            dma((3,)), dma((3,)),
            dma((ep_count,)), dma((ep_count,)),
            dma((3, ep_count)), dma((3, ep_count)),
            dma((ep_count, 2)), dma((ep_count, 2)),
            dma((ep_count,)), dma((ep_count,)),
            dma((ep_count,)), dma((ep_count,)),
            dma((6,)), dma((6,)),
            dma((3,)), dma((3,)),
        ],
        compiler_params=pltpu.CompilerParams(
            collective_id=0, has_side_effects=True, vmem_limit_bytes=60 * 1024 * 1024
        ),
    )(normed, ranks, weights, mixed, stats, gain, shift, proj, gate, up, down)


def shifted(value, axis, steps):
    count = lax.axis_size(axis)
    leading, last = (max(0, -steps), min(count, count - steps))
    return lax.ppermute(value, axis, [(source, source + steps) for source in range(leading, last)])


def local(
    conv_input,
    conv_kernel,
    norm_gain,
    norm_shift,
    conv_proj,
    moe_input,
    moe_gain,
    routes,
    route_weights,
    gate_proj,
    up_proj,
    down_proj,
):
    tp_count = lax.axis_size("tp")
    ep_count = lax.axis_size("ep")
    local_rows, local_width = conv_input.shape
    reach = conv_kernel.shape[0] - 1
    history = shifted(conv_input[local_rows - reach :], "ep", 1)
    padded = jnp.concatenate([history, conv_input], axis=0)
    taps = conv_kernel.astype(jnp.float32)
    mixed = jnp.zeros((local_rows, local_width), jnp.float32)
    for offset in range(reach + 1):
        mixed = mixed + padded[offset : offset + local_rows].astype(jnp.float32) * taps[offset]
    row_sums, row_squares = jnp.sum(mixed, axis=1), jnp.sum(mixed * mixed, axis=1)
    moe_float = moe_input.astype(jnp.float32)
    normed = (
        moe_float
        * lax.rsqrt(jnp.mean(moe_float * moe_float, axis=1, keepdims=True) + 1e-06)
        * moe_gain
    ).astype(jnp.bfloat16)
    group_rows, top_count = routes.shape
    model_width = normed.shape[1]
    capacity = 2 * top_count * group_rows // ep_count
    share = capacity // tp_count
    direct = tp_count == 4 and share % 16 == 0 and ep_count % 2 == 0 and ep_count >= 8
    if direct:
        hops = jnp.array(hop_order(ep_count), jnp.int32)
        experts = (lax.axis_index("ep") + hops) % ep_count
    else:
        experts = jnp.arange(ep_count, dtype=jnp.int32)
    named = routes.T[None, :, :] == experts[:, None, None]
    hit = jnp.any(named, axis=1)
    weight = jnp.sum(jnp.where(named, route_weights.T[None, :, :], 0.0), axis=1)
    tokens = jnp.arange(group_rows, dtype=jnp.int32)
    before = (tokens[:, None] < tokens[None, :]).astype(jnp.bfloat16)
    rank = jnp.dot(hit.astype(jnp.bfloat16), before, preferred_element_type=jnp.float32).astype(
        jnp.int32
    )
    if direct:
        ranks = jnp.where(hit, rank, -1)
        idle = jnp.zeros((6, local_rows), jnp.float32)
        stats = jnp.concatenate([row_sums[None, :], row_squares[None, :], idle], axis=0)
        return run_exchange(
            normed, ranks, weight, mixed, stats, norm_gain[None, :], norm_shift[None, :],
            conv_proj, gate_proj[0], up_proj[0], down_proj[0], ep_count, share,
        )
    full_width = local_width * tp_count
    sums, squares = lax.psum((row_sums, row_squares), "tp")
    center = sums / full_width
    spread = jnp.maximum(squares / full_width - center * center, 0.0)
    scaled = (mixed - center[:, None]) * lax.rsqrt(spread[:, None] + 1e-05) * norm_gain + norm_shift
    activated = jax.nn.silu(scaled).astype(jnp.bfloat16)
    partial = jnp.dot(activated, conv_proj, preferred_element_type=jnp.float32).astype(jnp.bfloat16)
    first = lax.axis_index("tp") * share
    slots = first + jnp.arange(share, dtype=jnp.int32)
    held = hit[:, None, :] & (rank[:, None, :] == slots[None, :, None])
    pick = held.astype(jnp.bfloat16).reshape(ep_count * share, group_rows)
    scale = (
        jnp.where(held, weight[:, None, :], 0.0)
        .astype(jnp.bfloat16)
        .reshape(ep_count * share, group_rows)
    )
    conv_out = lax.psum_scatter(partial, "tp", scatter_dimension=0, tiled=True)
    group = lax.all_gather(normed, "tp", axis=0, tiled=True)
    outgoing = jnp.dot(pick, group, preferred_element_type=jnp.float32).astype(jnp.bfloat16)
    landed = lax.all_to_all(
        outgoing.reshape(ep_count, share, model_width), "ep", split_axis=0, concat_axis=0, tiled=True
    ).reshape(ep_count * share, model_width)
    incoming = lax.all_gather(landed, "tp", axis=0, tiled=True)
    gated = jax.nn.silu(jnp.dot(incoming, gate_proj[0], preferred_element_type=jnp.float32))
    hidden = (gated * jnp.dot(incoming, up_proj[0], preferred_element_type=jnp.float32)).astype(
        jnp.bfloat16
    )
    pieces = jnp.dot(hidden, down_proj[0], preferred_element_type=jnp.float32).astype(jnp.bfloat16)
    summed = lax.psum_scatter(pieces, "tp", scatter_dimension=0, tiled=True)
    returned = lax.all_to_all(
        summed.reshape(ep_count, share, model_width), "ep", split_axis=0, concat_axis=0, tiled=True
    ).reshape(ep_count * share, model_width)
    combined = lax.dot_general(
        scale, returned, (((0,), (0,)), ((), ())), preferred_element_type=jnp.float32
    )
    moe_out = lax.psum_scatter(combined.astype(jnp.bfloat16), "tp", scatter_dimension=0, tiled=True)
    return (conv_out, moe_out)


def solution(mesh):
    placed = (
        P("ep", "tp"),
        P(None, "tp"),
        P("tp"),
        P("tp"),
        P("tp", None),
        P(("ep", "tp"), None),
        P(),
        P("ep", None),
        P("ep", None),
        P("ep", None, "tp"),
        P("ep", None, "tp"),
        P("ep", "tp", None),
    )
    return jax.shard_map(
        local,
        mesh=mesh,
        in_specs=placed,
        out_specs=(P(("ep", "tp"), None), P(("ep", "tp"), None)),
        check_vma=False,
    )
```

profile of v0, /device:TPU:1, one launch (start us, length us, event | category | flops | bytes accessed | tf_op | source)
XLA Modules:
  0.0 283.9 jit_solution(17267089320711708579)
XLA Ops:
  7.2 0.0 copy-start
  7.2 0.0 all-gather.3.cloned.1.call-start
  7.2 1.2 fusion.45
  8.5 1.8 fusion.47
  10.3 0.0 all-gather.3.cloned.1.call-update
  10.3 0.0 all-gather.5.cloned.1.call-start
  10.4 0.7 fusion.52
  11.1 0.2 convolution_convert_fusion.3
  11.3 0.1 eq.43
  11.4 0.1 and.14
  11.5 0.1 and.16
  11.5 0.0 copy-start.4
  11.6 0.7 eq.45
  12.2 26.7 %all-gather.3.cloned.1.call-done = bf16[256,2048]{1,0:T(8,128)(2,1)} async-done(((bf16[64,2048]{1,0:T(8,128)(2,1)}), bf16[256,2048]{1,0:T(8,128)(2,1)}) %all-gather.3.cloned.1.call-update) | async-done | bytes 1048592 | tf_op jit(solution)/shard_map/all_gather | solution.py:457
  38.9 1.7 convolution_convert_fusion.2
  40.6 1.2 reshape.43
  41.9 40.9 %all_to_all.10 = bf16[64,4,2048]{2,1,0:T(4,128)(2,1)S(1)} all-to-all(bf16[64,4,2048]{2,1,0:T(4,128)(2,1)} %reshape.43), channel_id=1, replica_groups=mesh['ep'=64,'tp'=4] {'ep'}, dimensions={0} | all-to-all | bytes 2097152 | tf_op jit(solution)/shard_map/all_to_all | solution.py:459
  82.8 1.1 reshape.44
  83.8 0.0 all-gather.5.cloned.1.call-update
  83.9 0.0 reduce-scatter.6.cloned.1.call-start
  83.9 46.7 %all-gather.5.cloned.1.call-done = bf16[1024,2048]{1,0:T(8,128)(2,1)} async-done(((bf16[256,2048]{1,0:T(8,128)(2,1)}), bf16[1024,2048]{1,0:T(8,128)(2,1)}) %all-gather.5.cloned.1.call-update) | async-done | bytes 4194320 | tf_op jit(solution)/shard_map/all_gather | solution.py:462
  130.6 6.6 %fusion.2 = f32[1024,512]{1,0:T(8,128)} fusion(bf16[1024,2048]{1,0:T(8,128)(2,1)} %all-gather.5.cloned.1.call-done, bf16[1,2048,512]{2,1,0:T(8,128)(2,1)} %param.22), kind=kOutput, calls=%fused_computation.35 | convolution fusion | flops 2147483648 | bytes 8388608 | tf_op jit(solution)/shard_map/dot_general | solution.py:464
  137.2 10.1 %convolution_convert_fusion = bf16[1024,2048]{1,0:T(8,128)(2,1)} fusion(bf16[1,512,2048]{2,1,0:T(8,128)(2,1)S(1)} %copy-done, f32[1024,512]{1,0:T(8,128)} %fusion.2, bf16[1024,2048]{1,0:T(8,128)(2,1)} %all-gather.5.cloned.1.call-done, bf16[1,2048,512]{2,1,0:T(8,128)(2,1)} %param.21), kind=kOutput, calls=%fused_computation.29 | convolution fusion | flops 4300210176 | bytes 14680064 | tf_op jit(solution)/shard_map/dot_general | solution.py:467
  147.3 0.0 reduce-scatter.6.cloned.1.call-update
  147.3 0.0 copy-start.7
  147.3 0.0 copy-start.8
  147.3 0.0 reduce-scatter.4.cloned.1.call-start
  147.4 1.1 copy-done.1
  148.5 3.8 %collective-permute-start = (bf16[30,512]{1,0:T(8,128)(2,1)S(1)}, bf16[30,512]{1,0:T(8,128)(2,1)S(1)}, u32[]{:S(2)}, u32[]{:S(2)}) collective-permute-start(bf16[30,512]{1,0:T(8,128)(2,1)S(1)} %slice.186), channel_id=1, source_target_pairs={{0,4},{4,8},{8,12},{12,16},{16,20},{20,24},{24,28},{28,32},{32,36}... | collective-permute-start | bytes 92168 | tf_op jit(solution)/shard_map/ppermute | solution.py:380
  152.4 0.9 collective-permute-done
  153.4 11.2 %fusion.55 = (f32[1024]{0:T(1024)S(1)}, f32[1024]{0:T(1024)S(1)}, f32[1024,512]{1,0:T(8,128)}) fusion(f32[512]{0:T(512)S(1)} %bitcast.87, bf16[1024,512]{1,0:T(8,128)(2,1)S(1)} %copy-done.1, f32[512]{0:T(512)S(1)} %bitcast.86, bf16[30,512]{1,0:T(8,128)(2,1)S(1)} %collective-permute-done, f32[512]{0:T(512)S(1)} %bitcast.85, f32[512]{0:T(512)S(1)} %bitcast.84, ...), kind=kLoop, calls=%fused_computation.104 | loop fusion | flops 96991232 | bytes 3248128 | tf_op jit(solution)/shard_map/reduce_sum | solution.py:407
  164.5 8.3 %all-reduce = (f32[1024]{0:T(1024)S(1)}, f32[1024]{0:T(1024)S(1)}) all-reduce(f32[1024]{0:T(1024)S(1)} %get-tuple-element.3, f32[1024]{0:T(1024)S(1)} %get-tuple-element.2), channel_id=1, replica_groups=mesh['ep'=64,'tp'=4] {'tp'}, use_global_device_ids=true, to_apply=%region_3.0 | all-reduce | flops 2048 | bytes 16384 | tf_op jit(solution)/shard_map/psum | solution.py:441
  172.9 0.0 copy-done.7
  172.9 0.0 copy-done.8
  172.9 6.9 %convolution_convert_fusion.1 = bf16[1024,2048]{1,0:T(8,128)(2,1)} fusion(bf16[512,2048]{1,0:T(8,128)(2,1)} %param.16, f32[1024,512]{1,0:T(8,128)} %get-tuple-element.6, f32[512]{0:T(512)S(1)} %copy-done.7, f32[512]{0:T(512)S(1)} %copy-done.8, f32[1024]{0:T(1024)S(1)} %get-tuple-element.39, f32[1024]{0:T(1024)S(1)} %get-tuple-element.38), kind=kOutput, calls=%fused_computation.30 | convolution fusion | flops 2154299392 | bytes 8400896 | tf_op jit(solution)/shard_map/dot_general | solution.py:446
  179.7 0.0 reduce-scatter.4.cloned.1.call-update
  179.8 0.0 copy-start.3
  179.8 0.0 copy-start.6
  179.8 17.9 %reduce-scatter.6.cloned.1.call-done = bf16[256,2048]{1,0:T(8,128)(2,1)} async-done(((bf16[1024,2048]{1,0:T(8,128)(2,1)}), bf16[256,2048]{1,0:T(8,128)(2,1)}) %reduce-scatter.6.cloned.1.call-update) | async-done | bytes 1048592 | tf_op jit(solution)/shard_map/reduce_scatter | solution.py:468
  197.7 2.2 reshape.45
  199.9 10.9 %all-to-all-start.1 = ((bf16[64,4,2048]{2,1,0:T(4,128)(2,1)}), bf16[64,4,2048]{2,1,0:T(4,128)(2,1)S(1)}, u32[]{:S(2)}, u32[]{:S(2)}) async-start(bf16[64,4,2048]{2,1,0:T(4,128)(2,1)} %reshape.45), calls=%async_computation.3 | async-start | bytes 2097152 | tf_op jit(solution)/shard_map/all_to_all | solution.py:469
  210.8 0.0 reduce-scatter.8.cloned.1.call-start
  211.0 0.2 select_convert_fusion
  211.2 27.9 %all-to-all-done.1 = bf16[64,4,2048]{2,1,0:T(4,128)(2,1)S(1)} async-done(((bf16[64,4,2048]{2,1,0:T(4,128)(2,1)}), bf16[64,4,2048]{2,1,0:T(4,128)(2,1)S(1)}, u32[]{:S(2)}, u32[]{:S(2)}) %all-to-all-start.1) | async-done | bytes 1048608 | tf_op jit(solution)/shard_map/all_to_all | solution.py:469
  239.0 2.4 fusion
  241.4 0.0 reduce-scatter.8.cloned.1.call-update
  241.4 8.3 %reduce-scatter.4.cloned.1.call-done = bf16[256,2048]{1,0:T(8,128)(2,1)} async-done(((bf16[1024,2048]{1,0:T(8,128)(2,1)}), bf16[256,2048]{1,0:T(8,128)(2,1)}) %reduce-scatter.4.cloned.1.call-update) | async-done | bytes 1048592 | tf_op jit(solution)/shard_map/reduce_scatter | solution.py:456
  249.7 27.7 %reduce-scatter.8.cloned.1.call-done = bf16[64,2048]{1,0:T(8,128)(2,1)} async-done(((bf16[256,2048]{1,0:T(8,128)(2,1)}), bf16[64,2048]{1,0:T(8,128)(2,1)}) %reduce-scatter.8.cloned.1.call-update) | async-done | bytes 262160 | tf_op jit(solution)/shard_map/reduce_scatter | solution.py:475
  (18 shorter events, 0.2 us)
Async XLA Ops:
  7.2 130.0 %copy-start = (bf16[1,512,2048]{2,1,0:T(8,128)(2,1)S(1)}, bf16[1,512,2048]{2,1,0:T(8,128)(2,1)}, u32[]{:S(2)}) copy-start(bf16[1,512,2048]{2,1,0:T(8,128)(2,1)} %param.23) | copy-start | bytes 6291460
  7.2 31.7 %all-gather.3.cloned.1.call-start = ((), (), s32[]{:S(2)}) async-start(), calls=%async_computation.6 | async-start | bytes 1310720 | tf_op jit(solution)/shard_map/all_gather | solution.py:457
  10.3 120.3 %all-gather.5.cloned.1.call-start = ((), (), s32[]{:S(2)}) async-start(), calls=%async_computation.7 | async-start | bytes 5242880 | tf_op jit(solution)/shard_map/all_gather | solution.py:462
  11.5 0.7 copy-start.4
  83.9 113.8 %reduce-scatter.6.cloned.1.call-start = ((), (), s32[]{:S(2)}) async-start(), calls=%async_computation.8 | async-start | bytes 5242880 | tf_op jit(solution)/shard_map/reduce_scatter | solution.py:468
  147.3 1.2 copy-start.1
  147.3 5.1 %copy-start.2 = (bf16[31,512]{1,0:T(8,128)(2,1)S(1)}, bf16[31,512]{1,0:T(8,128)(2,1)}, u32[]{:S(2)}) copy-start(bf16[31,512]{1,0:T(8,128)(2,1)} %param.13) | copy-start | bytes 95236
  147.3 25.6 %copy-start.7 = (f32[512]{0:T(512)S(1)}, f32[512]{0:T(512)}, u32[]{:S(2)}) copy-start(f32[512]{0:T(512)} %param.15) | copy-start | bytes 6148
  147.3 25.6 %copy-start.8 = (f32[512]{0:T(512)S(1)}, f32[512]{0:T(512)}, u32[]{:S(2)}) copy-start(f32[512]{0:T(512)} %param.14) | copy-start | bytes 6148
  147.3 102.4 %reduce-scatter.4.cloned.1.call-start = ((), (), s32[]{:S(2)}) async-start(), calls=%async_computation.5 | async-start | bytes 5242880 | tf_op jit(solution)/shard_map/reduce_scatter | solution.py:456
  148.5 4.8 %collective-permute-start = (bf16[30,512]{1,0:T(8,128)(2,1)S(1)}, bf16[30,512]{1,0:T(8,128)(2,1)S(1)}, u32[]{:S(2)}, u32[]{:S(2)}) collective-permute-start(bf16[30,512]{1,0:T(8,128)(2,1)S(1)} %slice.186), channel_id=1, source_target_pairs={{0,4},{4,8},{8,12},{12,16},{16,20},{20,24},{24,28},{28,32},{32,36}... | collective-permute-start | bytes 92168 | tf_op jit(solution)/shard_map/ppermute | solution.py:380
  179.8 31.1 %copy-start.3 = (s32[256,2]{0,1:T(2,128)S(1)}, s32[256,2]{0,1:T(2,128)}, u32[]{:S(2)}) copy-start(s32[256,2]{0,1:T(2,128)} %param.19) | copy-start | bytes 6148
  179.8 31.1 %copy-start.6 = (f32[256,2]{0,1:T(2,128)S(1)}, f32[256,2]{0,1:T(2,128)}, u32[]{:S(2)}) copy-start(f32[256,2]{0,1:T(2,128)} %param.20) | copy-start | bytes 6148
  179.8 31.1 %copy-start.5 = (s32[4]{0:T(128)S(1)}, s32[4]{0:T(128)}, u32[]{:S(2)}) copy-start(s32[4]{0:T(128)} %copy-done.4) | copy-start | bytes 52
  199.9 39.1 %all-to-all-start.1 = ((bf16[64,4,2048]{2,1,0:T(4,128)(2,1)}), bf16[64,4,2048]{2,1,0:T(4,128)(2,1)S(1)}, u32[]{:S(2)}, u32[]{:S(2)}) async-start(bf16[64,4,2048]{2,1,0:T(4,128)(2,1)} %reshape.45), calls=%async_computation.3 | async-start | bytes 2097152 | tf_op jit(solution)/shard_map/all_to_all | solution.py:469
  210.8 66.5 %reduce-scatter.8.cloned.1.call-start = ((), (), s32[]{:S(2)}) async-start(), calls=%async_computation.9 | async-start | bytes 1310720 | tf_op jit(solution)/shard_map/reduce_scatter | solution.py:475
Sparse Core Ops, SparseCore 0:
  10.4 28.4 all-gather.2
  84.0 46.5 all-gather.4
  147.4 50.2 reduce-scatter.5
  200.7 48.9 reduce-scatter.3
  252.6 24.6 reduce-scatter.7
where the time goes:
time: 285 us; the launch traced here: 284 us
  waiting for transfers between devices  156 us (55%)
  blocking collectives  49.2 us (17%)
  matrix products  27.8 us (10%)
  other arithmetic  15.2 us (5%)
  starting transfers between devices  15 us (5%)
  between operations  14 us (5%)
  local copies, waits for them, and re-layouts  6.72 us (2%)
    all_gather x1, waiting for transfers between devices, local(): incoming = lax.all_gather(landed, 'tp', axis=0, tiled=True)  46.7 us
    all_to_all x1, blocking collectives, local(): lax.all_to_all(outgoing.reshape(ep_count, share, model_width), 'ep', spli...  40.9 us
    all_to_all x1, waiting for transfers between devices, local(): lax.all_to_all(summed.reshape(ep_count, share, model_width), 'ep', split_...  27.9 us
    reduce_scatter x1, waiting for transfers between devices, local(): lax.psum_scatter(combined.astype(jnp.bfloat16), 'tp', scatter_dimension=0...  27.7 us
    all_gather x1, waiting for transfers between devices, local(): group = lax.all_gather(normed, 'tp', axis=0, tiled=True)  26.7 us
    reduce_scatter x1, waiting for transfers between devices, local(): summed = lax.psum_scatter(pieces, 'tp', scatter_dimension=0, tiled=True)  17.9 us
    reduce_sum x1, other arithmetic, local(): jnp.sum(mixed, axis=1)  11.2 us
    all_to_all x1, starting transfers between devices, local(): lax.all_to_all(summed.reshape(ep_count, share, model_width), 'ep', split_...  10.9 us
  transfers between devices with their start and end apart: 7, of which 7 were waited for; matrix products, arithmetic and copies ran while one was open for 9% of the time, Pallas kernels for 0%

commit v1 on v0

v1 whole, which is shorter than its diff:
```python
import functools

import jax
import jax.numpy as jnp
from jax import lax
from jax.experimental import pallas as pl
from jax.experimental.pallas import tpu as pltpu
from jax.sharding import PartitionSpec as P

MESH = pl.DeviceIdType.MESH
DIMS = (8, 4, 2)
f32, bf16, i32 = jnp.float32, jnp.bfloat16, jnp.int32


def layer(
    moe_in, moe_gain, routes, weights, taps_in, gain, shift, conv_hbm, proj_hbm, gate_hbm, up_hbm, down_hbm,
    conv_out, moe_out,
    padded, taps, mixed, sums, stats, stats_in, columns, proj, partial,
    conv_a, conv_b, conv_c, conv_d, conv_u, conv_v, history,
    gate, up, down, own, group, ranks, held_w, scale, outgoing, arrived, pieces,
    moe_a, moe_b, moe_c, moe_d, moe_u, moe_v, back_out, returned, combined, final,
    load_sem, hist_send, hist_recv, stat_send, stat_recv, a2a_send, a2a_recv, ep_send, ep_recv,
    gather_send, gather_recv, ret_send, ret_recv, back_send, back_recv, conv_send, conv_recv, fin_send, fin_recv,
    *, dims, cap,
):
    zs, xs, cs = dims
    ep_count = zs * xs * cs
    per = xs * cs
    chunk = per * cap
    rows, width = moe_in.shape
    col = width // 4
    half = col // 2
    conv_rows = conv_hbm.shape[0]
    conv_width = conv_hbm.shape[1]
    reach = taps_in.shape[0] - 1
    lead = 32
    span = conv_rows // 4
    tile = span // 2
    subs = 4
    sub = span // subs
    wide = width // 2

    me_ep, me = lax.axis_index("ep"), lax.axis_index("tp")
    core = lax.rem(me_ep, cs)
    mx = lax.rem(lax.div(me_ep, cs), xs)
    mz = lax.div(me_ep, cs * xs)
    nxt, prv = lax.rem(me + 1, 4), lax.rem(me + 3, 4)
    opp = lax.rem(me + 2, 4)

    def remote(src, dst, send, recv, where):
        return pltpu.make_async_remote_copy(
            src_ref=src, dst_ref=dst, send_sem=send, recv_sem=recv, device_id=where,
            device_id_type=MESH,
        )

    def aligned(start, size):
        return pl.ds(pl.multiple_of(start, size), size)

    def depth(c):
        t = lax.rem(c + 1, zs)
        sign = lax.rem(t, 2) * 2 - 1
        return sign * lax.div(t + 1, 2)

    def partner(c, j, way):
        dx, dc = j // cs, j % cs
        z = lax.rem(mz + way * depth(c) + zs, zs)
        x = lax.rem(mx + way * dx + xs, xs)
        return (z * xs + x) * cs + lax.rem(core + dc, cs)

    loads = [pltpu.make_async_copy(conv_hbm, padded.at[lead:], load_sem.at[0])]
    loads.append(pltpu.make_async_copy(proj_hbm, proj, load_sem.at[1]))
    for k in range(4):
        at = lax.rem(me + k, 4) * col
        loads.append(pltpu.make_async_copy(gate_hbm.at[0, aligned(at, col), :], gate.at[k], load_sem.at[2 + k]))
        loads.append(pltpu.make_async_copy(up_hbm.at[0, aligned(at, col), :], up.at[k], load_sem.at[6 + k]))
        loads.append(pltpu.make_async_copy(down_hbm.at[0, :, aligned(at, col)], down.at[k], load_sem.at[10 + k]))
    for load in loads:
        load.start()

    barrier = pltpu.get_barrier_semaphore()
    for k in range(1, 4):
        pl.semaphore_signal(barrier, inc=1, device_id={"tp": lax.rem(me + k, 4)}, device_id_type=MESH)

    def greet(d, carry):
        pl.semaphore_signal(
            barrier, inc=1, device_id={"ep": lax.rem(me_ep + d, ep_count)}, device_id_type=MESH
        )
        return carry

    lax.fori_loop(1, ep_count, greet, 0)

    value = moe_in[...].astype(f32)
    normed = (
        value * lax.rsqrt(jnp.mean(value * value, axis=1, keepdims=True) + 1e-06) * moe_gain[...]
    ).astype(bf16)
    for b in range(5):
        own[b] = normed[:, (b % 4) * col : (b % 4 + 1) * col]

    group_rows = routes.shape[1]
    s_at = lax.broadcasted_iota(i32, (ep_count, group_rows), 0)
    per_bits, core_bits = per.bit_length() - 1, cs.bit_length() - 1
    t = ((s_at >> per_bits) + 1) & (zs - 1)
    dz = ((t & 1) * 2 - 1) * ((t + 1) >> 1)
    dx = (s_at & (per - 1)) >> core_bits
    dc = s_at & (cs - 1)
    expert = ((((mz + dz + zs) & (zs - 1)) * xs + ((mx + dx) & (xs - 1))) * cs) + ((core + dc) & (cs - 1))
    first, second = routes[0:1, :] == expert, routes[1:2, :] == expert
    hit = first | second
    before = (
        lax.broadcasted_iota(i32, (group_rows, group_rows), 0)
        < lax.broadcasted_iota(i32, (group_rows, group_rows), 1)
    )
    rank = jnp.dot(
        jnp.where(hit, 1.0, 0.0).astype(bf16), jnp.where(before, 1.0, 0.0).astype(bf16),
        preferred_element_type=f32,
    )
    ranks[...] = jnp.where(hit, rank, -1.0)
    held_w[...] = jnp.where(first, weights[0:1, :], 0.0) + jnp.where(second, weights[1:2, :], 0.0)
    taps[0 : reach + 1, :] = taps_in[...].astype(f32)

    pl.semaphore_wait(barrier, ep_count + 2)

    a2a = []
    for k in range(1, 4):
        to = lax.rem(me + k, 4)
        a2a.append(
            remote(
                own.at[pl.ds(to, 2)], group.at[:, aligned(me * rows, rows), :],
                a2a_send.at[k - 1], a2a_recv.at[k - 1], {"tp": to},
            )
        )
    for r in a2a:
        r.start()
    group[:, aligned(me * rows, rows), :] = own[pl.ds(me, 2)]
    loads[0].wait()
    hist = remote(
        padded.at[lead + conv_rows - lead : lead + conv_rows], history, hist_send, hist_recv,
        {"ep": lax.rem(me_ep + 1, ep_count)},
    )
    hist.start()

    lane, strip = 128, 64

    def conv_tile(i, carry):
        for h in range(tile // strip):
            r0 = pl.multiple_of(i * tile + h * strip, strip)
            one = jnp.zeros((strip, lane), f32)
            two = jnp.zeros((strip, lane), f32)
            for n in range(0, conv_width, lane):
                x = padded[pl.ds(r0, strip + lead), n : n + lane].astype(f32)
                out = None
                for phase in range(8):
                    acc = None
                    extra = 8 if phase else 0
                    for q in range(lead // 8 + 1):
                        tap = 8 * q + phase - (lead - reach)
                        if tap < 0 or tap > reach:
                            continue
                        term = x[8 * q : 8 * q + strip + extra] * taps[tap : tap + 1, n : n + lane]
                        acc = term if acc is None else acc + term
                    if acc is None:
                        continue
                    part = acc[phase : phase + strip]
                    out = part if out is None else out + part
                mixed[pl.ds(r0, strip), n : n + lane] = out
                one = one + out
                two = two + out * out
            sums[0, h * strip : (h + 1) * strip, :] = one
            sums[1, h * strip : (h + 1) * strip, :] = two
        for m in range(2):
            stats[m, pl.ds(i, 1), :] = jnp.sum(sums[m].T, axis=0, keepdims=True)
        return carry

    tiles = conv_rows // tile
    lax.fori_loop(1, 4, conv_tile, 0)

    for r in a2a:
        r.wait_recv()

    slot = lax.broadcasted_iota(i32, (cap, group_rows), 0).astype(f32)

    def ep_copy(c, j):
        s = c * per + j
        return remote(
            outgoing.at[:, aligned(s * cap, cap), :],
            arrived.at[0:2, aligned(s * cap, cap), :],
            ep_send.at[s], ep_recv.at[s], {"ep": partner(c, j, 1)},
        )

    def dispatch(c, carry):
        ranked = ranks[aligned(c * per, per), :]
        pick = jnp.concatenate(
            [jnp.where(ranked[j : j + 1, :] == slot, 1.0, 0.0) for j in range(per)], axis=0
        ).astype(bf16)
        here = aligned(c * chunk, chunk)
        for b in range(2):
            outgoing[b, here, :] = jnp.dot(pick, group[b], preferred_element_type=f32).astype(bf16)

        for j in range(per):
            if j == 0:
                @pl.when(c < zs - 1)
                def _():
                    ep_copy(c, 0).start()
            else:
                ep_copy(c, j).start()
        return carry

    lax.fori_loop(0, zs, dispatch, 0)
    mine = slice((zs - 1) * chunk, (zs - 1) * chunk + cap)
    arrived[0:2, mine, :] = outgoing[:, mine, :]

    lax.fori_loop(4, tiles, conv_tile, 0)
    hist.wait_recv()
    padded[0:lead, :] = jnp.where(me_ep == 0, jnp.zeros((lead, conv_width), bf16), history[...])
    lax.fori_loop(0, 1, conv_tile, 0)

    moments = [
        remote(stats, stats_in.at[k - 1], stat_send.at[k - 1], stat_recv.at[k - 1], {"tp": lax.rem(me + k, 4)})
        for k in range(1, 4)
    ]
    for r in moments:
        r.start()

    def weigh(c, carry):
        ranked = ranks[aligned(c * per, per), :]
        held = held_w[aligned(c * per, per), :]
        block = jnp.concatenate(
            [jnp.where(ranked[j : j + 1, :] == slot, held[j : j + 1, :], 0.0) for j in range(per)], axis=0
        )
        scale[c] = block.T.astype(bf16)
        return carry

    lax.fori_loop(0, zs, weigh, 0)

    def center_and_scale():
        for r in moments:
            r.wait_recv()
        total = (stats[...] + stats_in[0] + stats_in[1] + stats_in[2]) / width
        center = total[0]
        spread = jnp.maximum(total[1] - center * center, 0.0)
        inverse = lax.rsqrt(spread + 1e-05)
        for i in range(tiles):
            both = jnp.concatenate([center[i : i + 1], inverse[i : i + 1]] + [center[i : i + 1]] * 6, axis=0)
            columns[i * tile : (i + 1) * tile, :] = both.T

    step_cols = min(512, width)

    def project(k, h):
        at = lax.rem(me + k, 4) * span + h * tile
        view = aligned(at, tile)
        stat = columns[view, :]
        scaled = (mixed[view, :] - stat[:, 0:1]) * stat[:, 1:2] * gain[...] + shift[...]
        activated = (scaled / (1.0 + jnp.exp(-scaled))).astype(bf16)
        for n in range(0, width, step_cols):
            partial[k, aligned(h * tile, tile), n : n + step_cols] = jnp.dot(
                activated, proj[:, n : n + step_cols], preferred_element_type=f32
            ).astype(bf16)

    def conv_copies(j):
        at = aligned(j * sub, sub)
        low, high = slice(0, wide), slice(wide, width)

        def one(n, src, dst, where):
            return remote(src, dst, conv_send.at[n, j], conv_recv.at[n, j], {"tp": where})

        return [
            one(0, partial.at[2, at, low], conv_a.at[at, :], nxt),
            one(1, partial.at[2, at, high], conv_b.at[at, :], prv),
            one(2, partial.at[1, at, high], conv_c.at[at, high], nxt),
            one(3, partial.at[3, at, low], conv_d.at[at, low], prv),
            one(4, conv_u.at[at, :], conv_c.at[at, low], nxt),
            one(5, conv_v.at[at, :], conv_d.at[at, high], prv),
        ]

    def conv_first(j):
        for r in conv_copies(j)[:4]:
            r.start()

    def conv_second(j):
        copies = conv_copies(j)
        at = aligned(j * sub, sub)
        copies[0].wait_recv()
        conv_u[at, :] = (partial[1, at, :wide].astype(f32) + conv_a[at, :].astype(f32)).astype(bf16)
        copies[4].start()
        copies[1].wait_recv()
        conv_v[at, :] = (partial[3, at, wide:].astype(f32) + conv_b[at, :].astype(f32)).astype(bf16)
        copies[5].start()

    def conv_last(j, carry):
        copies = conv_copies(j)
        at = aligned(j * sub, sub)
        for n in (2, 3, 4, 5):
            copies[n].wait_recv()
        conv_out[at, :] = (
            partial[0, at, :].astype(f32) + conv_c[at, :].astype(f32) + conv_d[at, :].astype(f32)
        ).astype(bf16)
        return carry

    def gather_copies(c):
        at = aligned(c * chunk, chunk)
        return [
            remote(arrived.at[1, at, :], arrived.at[2, at, :], gather_send.at[0, c], gather_recv.at[0, c], {"tp": prv}),
            remote(arrived.at[0, at, :], arrived.at[3, at, :], gather_send.at[1, c], gather_recv.at[1, c], {"tp": nxt}),
        ]

    def land(c):
        for j in range(per):
            if j == 0:
                @pl.when(c < zs - 1)
                def _():
                    ep_copy(c, 0).wait_recv()
            else:
                ep_copy(c, j).wait_recv()
        for r in gather_copies(c):
            r.start()

    def return_copies(c):
        at = aligned(c * chunk, chunk)
        low, high = slice(0, half), slice(half, col)

        def one(n, src, dst, where):
            return remote(src, dst, ret_send.at[n, c], ret_recv.at[n, c], {"tp": where})

        return [
            one(0, pieces.at[2, at, low], moe_a.at[at, :], nxt),
            one(1, pieces.at[2, at, high], moe_b.at[at, :], prv),
            one(2, pieces.at[1, at, high], moe_c.at[at, high], nxt),
            one(3, pieces.at[3, at, low], moe_d.at[at, low], prv),
            one(4, moe_u.at[at, :], moe_c.at[at, low], nxt),
            one(5, moe_v.at[at, :], moe_d.at[at, high], prv),
        ]

    def experts(c):
        for r in gather_copies(c):
            r.wait_recv()
        at = aligned(c * chunk, chunk)
        lines = [arrived[k, at, :] for k in range(4)]
        hidden = []
        step = min(256, col)
        for n in range(0, col, step):
            left = sum(jnp.dot(lines[k], gate[k, :, n : n + step], preferred_element_type=f32) for k in range(4))
            right = sum(jnp.dot(lines[k], up[k, :, n : n + step], preferred_element_type=f32) for k in range(4))
            hidden.append((left / (1.0 + jnp.exp(-left)) * right).astype(bf16))
        hid = jnp.concatenate(hidden, axis=1)
        for k in (2, 1, 3, 0):
            pieces[k, at, :] = jnp.dot(hid, down[k], preferred_element_type=f32).astype(bf16)
        for r in return_copies(c)[:4]:
            r.start()

    def middle(c):
        copies = return_copies(c)
        at = aligned(c * chunk, chunk)
        copies[0].wait_recv()
        moe_u[at, :] = (pieces[1, at, :half].astype(f32) + moe_a[at, :].astype(f32)).astype(bf16)
        copies[4].start()
        copies[1].wait_recv()
        moe_v[at, :] = (pieces[3, at, half:].astype(f32) + moe_b[at, :].astype(f32)).astype(bf16)
        copies[5].start()

    def back_copy(c, j):
        s = c * per + j
        at = aligned(s * cap, cap)
        return remote(
            back_out.at[at, :], returned.at[at, :], back_send.at[s], back_recv.at[s],
            {"ep": partner(c, j, -1)},
        )

    def finish(c):
        copies = return_copies(c)
        at = aligned(c * chunk, chunk)
        for n in (2, 3, 4, 5):
            copies[n].wait_recv()
        back_out[at, :] = (
            pieces[0, at, :].astype(f32) + moe_c[at, :].astype(f32) + moe_d[at, :].astype(f32)
        ).astype(bf16)
        for j in range(per):
            if j == 0:
                @pl.when(c < zs - 1)
                def _():
                    back_copy(c, 0).start()
            else:
                back_copy(c, j).start()

    def step(i, carry):
        @pl.when(i < zs)
        def _():
            land(i)

        @pl.when(i == 0)
        def _():
            center_and_scale()
            loads[1].wait()

        @pl.when(i < 2)
        def _():
            def both(h, inner):
                project(2 + i, h)
                project(1 - i, h)
                return inner

            lax.fori_loop(0, 2, both, 0)

        @pl.when((i >= 2) & (i < 2 + subs))
        def _():
            conv_first(i - 2)

        @pl.when((i >= 1) & (i <= zs))
        def _():
            middle(i - 1)

        @pl.when((i >= 3) & (i < 3 + subs))
        def _():
            conv_second(i - 3)

        @pl.when((i >= 2) & (i < zs + 2))
        def _():
            finish(i - 2)

        @pl.when(i == 0)
        def _():
            for load in loads[2:]:
                load.wait()

        @pl.when(i < zs)
        def _():
            experts(i)

        return carry

    lax.fori_loop(0, max(zs + 2, subs + 3), step, 0)
    lax.fori_loop(0, subs, conv_last, 0)

    returned[mine, :] = back_out[mine, :]
    total = jnp.zeros((group_rows, col), f32)
    for c in range(zs):
        for j in range(per):
            if (c, j) != (zs - 1, 0):
                back_copy(c, j).wait_recv()
        total = total + jnp.dot(
            scale[c], returned[c * chunk : (c + 1) * chunk, :], preferred_element_type=f32
        )
    combined[...] = total.astype(bf16)
    last = []
    for k in range(1, 4):
        to = lax.rem(me + k, 4)
        last.append(
            remote(
                combined.at[aligned(to * rows, rows), :], final.at[me],
                fin_send.at[k - 1], fin_recv.at[k - 1], {"tp": to},
            )
        )
    for r in last:
        r.start()
    final[me] = combined[aligned(me * rows, rows), :]
    for r in last:
        r.wait_recv()
    for b in range(4):
        moe_out[:, b * col : (b + 1) * col] = final[b]

    for r in a2a + [hist] + moments + last:
        r.wait_send()

    def drain(c, carry):
        for j in range(per):
            if j == 0:
                @pl.when(c < zs - 1)
                def _():
                    ep_copy(c, 0).wait_send()
                    back_copy(c, 0).wait_send()
            else:
                ep_copy(c, j).wait_send()
                back_copy(c, j).wait_send()
        for r in gather_copies(c) + return_copies(c):
            r.wait_send()
        return carry

    lax.fori_loop(0, zs, drain, 0)

    def conv_drain(j, carry):
        for r in conv_copies(j):
            r.wait_send()
        return carry

    lax.fori_loop(0, subs, conv_drain, 0)


def local(
    conv_input, conv_kernel, norm_gain, norm_shift, conv_proj, moe_input, moe_gain,
    routes, route_weights, gate_proj, up_proj, down_proj, *, dims=DIMS,
):
    zs, xs, cs = dims
    ep_count = zs * xs * cs
    conv_rows, conv_width = conv_input.shape
    rows, width = moe_input.shape
    group_rows = routes.shape[0]
    cap = 16
    slots = ep_count * cap
    col, half, wide = width // 4, width // 8, width // 2
    span = conv_rows // 4
    tile = span // 2
    tiles = conv_rows // tile
    hid = gate_proj.shape[2]
    chunk = xs * cs * cap
    reach = conv_kernel.shape[0] - 1
    vmem, dma = pltpu.VMEM, pltpu.SemaphoreType.DMA
    at_vmem, at_any = pl.BlockSpec(memory_space=pltpu.VMEM), pl.BlockSpec(memory_space=pl.ANY)
    scratch = [
        vmem((32 + conv_rows, conv_width), bf16),
        vmem((32, conv_width), f32),
        vmem((conv_rows, conv_width), f32),
        vmem((2, tile, 128), f32),
        vmem((2, tiles, tile), f32),
        vmem((3, 2, tiles, tile), f32),
        vmem((conv_rows, 8), f32),
        vmem((conv_width, width), bf16),
        vmem((4, span, width), bf16),
        vmem((span, wide), bf16), vmem((span, wide), bf16),
        vmem((span, width), bf16), vmem((span, width), bf16),
        vmem((span, wide), bf16), vmem((span, wide), bf16),
        vmem((32, conv_width), bf16),
        vmem((4, col, hid), bf16), vmem((4, col, hid), bf16), vmem((4, hid, col), bf16),
        vmem((5, rows, col), bf16),
        vmem((2, group_rows, col), bf16),
        vmem((ep_count, group_rows), f32), vmem((ep_count, group_rows), f32),
        vmem((zs, group_rows, chunk), bf16),
        vmem((2, slots, col), bf16),
        vmem((4, slots, col), bf16),
        vmem((4, slots, col), bf16),
        vmem((slots, half), bf16), vmem((slots, half), bf16),
        vmem((slots, col), bf16), vmem((slots, col), bf16),
        vmem((slots, half), bf16), vmem((slots, half), bf16),
        vmem((slots, col), bf16), vmem((slots, col), bf16),
        vmem((group_rows, col), bf16),
        vmem((4, rows, col), bf16),
        dma((14,)),
        dma, dma,
        dma((3,)), dma((3,)),
        dma((3,)), dma((3,)),
        dma((ep_count,)), dma((ep_count,)),
        dma((2, zs)), dma((2, zs)),
        dma((6, zs)), dma((6, zs)),
        dma((ep_count,)), dma((ep_count,)),
        dma((6, 4)), dma((6, 4)),
        dma((3,)), dma((3,)),
    ]
    return pl.pallas_call(
        functools.partial(layer, dims=dims, cap=cap),
        out_shape=(
            jax.ShapeDtypeStruct((span, width), bf16),
            jax.ShapeDtypeStruct((rows, width), bf16),
        ),
        in_specs=[at_vmem] * 7 + [at_any] * 5,
        out_specs=(at_vmem, at_vmem),
        scratch_shapes=scratch,
        compiler_params=pltpu.CompilerParams(
            collective_id=0, has_side_effects=True, vmem_limit_bytes=60 * 1024 * 1024
        ),
    )(
        moe_input, moe_gain[None, :], routes.T, route_weights.T, conv_kernel, norm_gain[None, :],
        norm_shift[None, :], conv_input, conv_proj, gate_proj, up_proj, down_proj,
    )


def solution(mesh):
    placed = (
        P("ep", "tp"),
        P(None, "tp"),
        P("tp"),
        P("tp"),
        P("tp", None),
        P(("ep", "tp"), None),
        P(),
        P("ep", None),
        P("ep", None),
        P("ep", None, "tp"),
        P("ep", None, "tp"),
        P("ep", "tp", None),
    )
    return jax.shard_map(
        local,
        mesh=mesh,
        in_specs=placed,
        out_specs=(P(("ep", "tp"), None), P(("ep", "tp"), None)),
        check_vma=False,
    )
```

time: 285 us -> 154 us (0.54)
  waiting for transfers between devices: 156 us -> 0 us
  Pallas kernels: 0 us -> 150 us
  blocking collectives: 49.2 us -> 0 us
  matrix products: 27.8 us -> 0 us
  other arithmetic: 15.2 us -> 0 us
  starting transfers between devices: 15 us -> 0 us
  between operations: 14 us -> 0.65 us
  local copies, waits for them, and re-layouts: 6.72 us -> 3.05 us
    pallas_call x0 -> x1, Pallas kernels: none -> 150 us  [local(): pl.pallas_call(functools.partial(layer, dims=dims, cap=cap), out_shape=(j...]
    all_gather x2 -> x0, waiting for transfers between devices: 73.4 us -> none  [the longest x1 46.7 us: local(): incoming = lax.all_gather(landed, 'tp', axis=0, tiled=True)]
    reduce_scatter x3 -> x0, waiting for transfers between devices: 53.8 us -> none  [the longest x1 27.7 us: local(): lax.psum_scatter(combined.astype(jnp.bfloat16), 'tp', scatter_dimension=0...]
    all_to_all x1 -> x0, blocking collectives: 40.9 us -> none  [local(): lax.all_to_all(outgoing.reshape(ep_count, share, model_width), 'ep', spli...]
    all_to_all x1 -> x0, waiting for transfers between devices: 27.9 us -> none  [local(): lax.all_to_all(summed.reshape(ep_count, share, model_width), 'ep', split_...]
    dot_general x6 -> x0, matrix products: 27.8 us -> none  [the longest x1 10.1 us: local(): jnp.dot(hidden, down_proj[0], preferred_element_type=jnp.float32)]
    reduce_sum x3 -> x0, other arithmetic: 12.5 us -> none  [the longest x1 11.2 us: local(): jnp.sum(mixed, axis=1)]
    all_to_all x1 -> x0, starting transfers between devices: 10.9 us -> none  [local(): lax.all_to_all(summed.reshape(ep_count, share, model_width), 'ep', split_...]
  transfers between devices with their start and end apart: 7 -> 0, of which waited for: 7 -> 0; matrix products, arithmetic and copies ran while one was open for 9% -> 0% of each run, Pallas kernels for 0% -> 0%
where the time goes in v1:
time: 154 us
  Pallas kernels  150 us (97%)
  local copies, waits for them, and re-layouts  3.05 us (2%)
    pallas_call x1, Pallas kernels, local(): pl.pallas_call(functools.partial(layer, dims=dims, cap=cap), out_shape=(j...  150 us

profile of v1, /device:TPU:1, one launch (start us, length us, event | category | flops | bytes accessed | tf_op | source)
XLA Modules:
  0.0 153.5 jit_solution(6806773232796253720)
XLA Ops:
  0.6 149.8 %shard_map.131 = (bf16[256,2048]{1,0:T(8,128)(2,1)}, bf16[64,2048]{1,0:T(8,128)(2,1)}) custom-call(bf16[64,2048]{1,0:T(8,128)(2,1)} %moe_in.1, f32[1,2048]{1,0:T(1,128)} %bitcast.5, s32[2,256]{1,0:T(2,128)} %bitcast.6, f32[2,256]{1,0:T(2,128)} %bitcast.7, bf16[31,512]{1,0:T(8,128)(2,1)} %taps_in.1, f32[1,512]{1,0:T(1,128)} %bitcast.8, f32[1,512]{1,0:T(1,128)} %bitcast.9, ...), custom_call_target="tpu_custom_call" | custom-call | tf_op jit(solution)/shard_map/pallas_call | solution.py:546
  150.5 0.0 copy-start
  150.5 2.3 %copy.16 = bf16[256,2048]{1,0:T(8,128)(2,1)} copy(bf16[256,2048]{1,0:T(8,128)(2,1)} %get-tuple-element.4) | data formatting | bytes 2097152
  152.8 0.0 copy-done
  152.8 0.7 copy.17
Async XLA Ops:
  150.5 2.4 %copy-start = (bf16[64,2048]{1,0:T(8,128)(2,1)S(1)}, bf16[64,2048]{1,0:T(8,128)(2,1)}, u32[]{:S(2)}) copy-start(bf16[64,2048]{1,0:T(8,128)(2,1)} %get-tuple-element.5) | copy-start | bytes 786436

commit v2 on v1

v2 whole, which is shorter than its diff:
```python
import functools

import jax
import jax.numpy as jnp
from jax import lax
from jax.experimental import pallas as pl
from jax.experimental.pallas import tpu as pltpu
from jax.sharding import PartitionSpec as P

MESH = pl.DeviceIdType.MESH
DIMS = (8, 4, 2)
f32, bf16, i32 = jnp.float32, jnp.bfloat16, jnp.int32


def layer(
    moe_in, moe_gain, routes, weights, taps_in, gain, shift, conv_hbm, proj_hbm, gate_hbm, up_hbm, down_hbm,
    conv_out, moe_out,
    padded, xin, history, taps_src, taps_all, taps, affine_src, affine, mixed, sums, act, wfull, conv_v,
    gate, up, down, own, group, ranks, held_w, scale, outgoing, arrived, pieces,
    moe_a, moe_b, moe_c, moe_d, moe_u, moe_v, back_out, returned, combined, final,
    load_sem, out_sem, ready, hist_send, hist_recv, relay_send, relay_recv, a2a_send, a2a_recv,
    cx_send, cx_recv, tap_send, tap_recv, aff_send, aff_recv,
    wy_send, wy_recv, wx_send, wx_recv, wd_send, wd_recv, ep_send, ep_recv,
    gather_send, gather_recv, ret_send, ret_recv, back_send, back_recv, fin_send, fin_recv,
    *, dims, cap,
):
    zs, xs, cs = dims
    ep_count = zs * xs * cs
    per = xs * cs
    chunk = per * cap
    rows, width = moe_in.shape
    col = width // 4
    half = col // 2
    conv_rows = conv_hbm.shape[0]
    conv_width = conv_hbm.shape[1]
    reach = taps_in.shape[0] - 1
    lead = 32
    span = conv_rows // 4
    slice_cols = width // per

    me_ep, me = lax.axis_index("ep"), lax.axis_index("tp")
    core = lax.rem(me_ep, cs)
    mx = lax.rem(lax.div(me_ep, cs), xs)
    mz = lax.div(me_ep, cs * xs)
    nxt, prv = lax.rem(me + 1, 4), lax.rem(me + 3, 4)

    def remote(src, dst, send, recv, where):
        return pltpu.make_async_remote_copy(
            src_ref=src, dst_ref=dst, send_sem=send, recv_sem=recv, device_id=where,
            device_id_type=MESH,
        )

    def aligned(start, size):
        return pl.ds(pl.multiple_of(start, size), size)

    def depth(c):
        t = c + lax.div(c + zs - 2, zs - 1) - (zs - 1) * lax.div(c, zs - 1)
        sign = lax.rem(t, 2) * 2 - 1
        return sign * lax.div(t + 1, 2)

    def place(z, x, c):
        return (z * xs + x) * cs + c

    def partner(c, j, way):
        dx, dc = j // cs, j % cs
        z = lax.rem(mz + way * depth(c) + zs, zs)
        x = lax.rem(mx + way * dx + xs, xs)
        return place(z, x, lax.rem(core + dc, cs))

    barrier = pltpu.get_barrier_semaphore()
    along_z = sorted(range(1, zs), key=lambda d: -min(d, zs - d))
    for d in along_z:
        pl.semaphore_signal(
            barrier, inc=1, device_id={"ep": place(lax.rem(mz + d, zs), mx, core)}, device_id_type=MESH
        )
    for k in (2, 1, 3):
        pl.semaphore_signal(barrier, inc=1, device_id={"tp": lax.rem(me + k, 4)}, device_id_type=MESH)
    for j in range(1, per):
        where = place(mz, lax.rem(mx + j // cs, xs), lax.rem(core + j % cs, cs))
        pl.semaphore_signal(barrier, inc=1, device_id={"ep": where}, device_id_type=MESH)

    loads = [pltpu.make_async_copy(conv_hbm, padded.at[lead:], load_sem.at[0])]
    proj_loads = [
        pltpu.make_async_copy(
            proj_hbm.at[:, q * slice_cols : (q + 1) * slice_cols], wfull.at[q, me], load_sem.at[13 + q]
        )
        for q in range(per)
    ]
    for k in range(4):
        at = lax.rem(me + k, 4) * col
        loads.append(pltpu.make_async_copy(gate_hbm.at[0, aligned(at, col), :], gate.at[k], load_sem.at[1 + k]))
        loads.append(pltpu.make_async_copy(up_hbm.at[0, aligned(at, col), :], up.at[k], load_sem.at[5 + k]))
        loads.append(pltpu.make_async_copy(down_hbm.at[0, :, aligned(at, col)], down.at[k], load_sem.at[9 + k]))
    for load in loads[:1] + proj_loads + loads[1:]:
        load.start()

    value = moe_in[...].astype(f32)
    normed = (
        value * lax.rsqrt(jnp.mean(value * value, axis=1, keepdims=True) + 1e-06) * moe_gain[...]
    ).astype(bf16)
    for b in range(5):
        own[b] = normed[:, (b % 4) * col : (b % 4 + 1) * col]

    group_rows = routes.shape[1]
    s_at = lax.broadcasted_iota(i32, (ep_count, group_rows), 0)
    per_bits, core_bits = per.bit_length() - 1, cs.bit_length() - 1
    c_at = s_at >> per_bits
    t = jnp.where(c_at == 0, 0, jnp.where(c_at == zs - 1, 1, c_at + 1))
    dz = ((t & 1) * 2 - 1) * ((t + 1) >> 1)
    dx = (s_at & (per - 1)) >> core_bits
    dc = s_at & (cs - 1)
    expert = ((((mz + dz + zs) & (zs - 1)) * xs + ((mx + dx) & (xs - 1))) * cs) + ((core + dc) & (cs - 1))
    first, second = routes[0:1, :] == expert, routes[1:2, :] == expert
    hit = first | second
    before = (
        lax.broadcasted_iota(i32, (group_rows, group_rows), 0)
        < lax.broadcasted_iota(i32, (group_rows, group_rows), 1)
    )
    rank = jnp.dot(
        jnp.where(hit, 1.0, 0.0).astype(bf16), jnp.where(before, 1.0, 0.0).astype(bf16),
        preferred_element_type=f32,
    )
    ranks[...] = jnp.where(hit, rank, -1.0)
    held_w[...] = jnp.where(first, weights[0:1, :], 0.0) + jnp.where(second, weights[1:2, :], 0.0)
    taps_src[...] = jnp.zeros_like(taps_src)
    taps_src[0 : reach + 1, :] = taps_in[...]
    affine_src[0:1, :] = gain[...]
    affine_src[1:2, :] = shift[...]
    padded[0:lead, :] = jnp.zeros((lead, conv_width), bf16)
    sums[...] = jnp.zeros_like(sums)

    pl.semaphore_wait(barrier, zs + per + 1)

    a2a, conv_x, params = [], [], []
    for k in range(1, 4):
        to = lax.rem(me + k, 4)
        a2a.append(
            remote(
                own.at[pl.ds(to, 2)], group.at[:, aligned(me * rows, rows), :],
                a2a_send.at[k - 1], a2a_recv.at[k - 1], {"tp": to},
            )
        )
        conv_x.append(
            remote(
                padded.at[pl.ds(pl.multiple_of(to * span, span), span + lead), :], xin.at[me],
                cx_send.at[k - 1], cx_recv.at[k - 1], {"tp": to},
            )
        )
        params.append(remote(taps_src, taps_all.at[me], tap_send.at[k - 1], tap_recv.at[k - 1], {"tp": to}))
        params.append(remote(affine_src, affine.at[me], aff_send.at[k - 1], aff_recv.at[k - 1], {"tp": to}))
    for r in a2a:
        r.start()
    for d in along_z:
        pl.semaphore_signal(
            ready, inc=1, device_id={"ep": place(lax.rem(mz + d, zs), mx, core)}, device_id_type=MESH
        )
    loads[0].wait()
    group[:, aligned(me * rows, rows), :] = own[pl.ds(me, 2)]
    xin[me] = padded[pl.ds(pl.multiple_of(me * span, span), span + lead), :]
    taps_all[me] = taps_src[...]
    affine[me] = affine_src[...]

    hist = remote(
        padded.at[conv_rows : conv_rows + lead], history.at[4], hist_send, hist_recv,
        {"ep": lax.rem(me_ep + 1, ep_count)},
    )

    def hist_relay(k):
        return remote(history.at[4], history.at[k], relay_send.at[k - 1], relay_recv.at[k - 1], {"tp": 0 * me})

    def pass_history():
        hist.wait_recv()
        for k in range(1, 4):
            @pl.when(me == k)
            def _():
                hist_relay(k).start()

    pl.semaphore_wait(ready, zs - 1)
    hist.start()

    lane, strip = 128, min(64, span)
    strips = span // strip

    def conv_block(b):
        def conv_strip(i, carry):
            at = aligned(i * strip, strip)
            r0 = pl.multiple_of(i * strip, strip)
            one = jnp.zeros((strip, lane), f32)
            two = jnp.zeros((strip, lane), f32)
            for n in range(0, conv_width, lane):
                x = xin[b, pl.ds(r0, strip + lead), n : n + lane].astype(f32)
                out = None
                for phase in range(8):
                    acc = None
                    extra = 8 if phase else 0
                    for q in range(lead // 8 + 1):
                        tap = 8 * q + phase - (lead - reach)
                        if tap < 0 or tap > reach:
                            continue
                        term = x[8 * q : 8 * q + strip + extra] * taps[b, tap : tap + 1, n : n + lane]
                        acc = term if acc is None else acc + term
                    if acc is None:
                        continue
                    part = acc[phase : phase + strip]
                    out = part if out is None else out + part
                mixed[b, at, n : n + lane] = out
                one = one + out
                two = two + out * out
            sums[0, at, :] = sums[0, at, :] + one
            sums[1, at, :] = sums[1, at, :] + two
            return carry

        lax.fori_loop(0, strips, conv_strip, 0)

    def normalise(i, carry):
        at = aligned(i * strip, strip)
        center = jnp.sum(sums[0, at, :], axis=1, keepdims=True) / width
        square = jnp.sum(sums[1, at, :], axis=1, keepdims=True) / width
        inverse = lax.rsqrt(jnp.maximum(square - center * center, 0.0) + 1e-05)
        for b in range(4):
            scaled = (mixed[b, at, :] - center) * inverse * affine[b, 0:1, :] + affine[b, 1:2, :]
            act[b, at, :] = (scaled / (1.0 + jnp.exp(-scaled))).astype(bf16)
        return carry

    def take_history(k):
        @pl.when(me == 0)
        def _():
            b = (4 - k) % 4
            if b:
                hist_relay(b).wait_recv()
            before_rows = history[4 if b == 0 else b]
            xin[b, 0:lead, :] = jnp.where(me_ep == 0, jnp.zeros_like(before_rows), before_rows)

    def convolve(k):
        b = lax.rem(me + 4 - k, 4)
        if k:
            params[2 * k - 2].wait_recv()
            params[2 * k - 1].wait_recv()
            conv_x[k - 1].wait_recv()
        taps[b] = taps_all[b].astype(f32)
        take_history(k)
        conv_block(b)

    slice_id = mx * cs + core

    def w_first(k):
        piece = wfull.at[slice_id, me]
        return remote(piece, piece, wy_send.at[k - 1], wy_recv.at[k - 1], {"tp": lax.rem(me + k, 4)})

    def w_along(k, d):
        piece = wfull.at[slice_id, lax.rem(me + 4 - k, 4)]
        return remote(
            piece, piece, wx_send.at[d - 1, k - 1], wx_recv.at[d - 1, k - 1],
            {"ep": place(mz, lax.rem(mx + d, xs), core)},
        )

    def w_across(k, d):
        piece = wfull.at[lax.rem(mx + xs - d, xs) * cs + core, lax.rem(me + 4 - k, 4)]
        return remote(
            piece, piece, wd_send.at[d, k - 1], wd_recv.at[d, k - 1],
            {"ep": place(mz, mx, lax.rem(core + 1, cs))},
        )

    def w_spread(k):
        w_first(k).wait_recv()
        for d in range(1, xs):
            w_along(k, d).start()
        if cs > 1:
            w_across(k, 0).start()

    def w_share(k):
        for d in range(1, xs):
            w_along(k, d).wait_recv()
            if cs > 1:
                w_across(k, d).start()

    def multiply(side):
        def one(d, carry):
            q = lax.rem(mx + d, xs) * cs + lax.rem(core + side, cs)
            total = sum(jnp.dot(act[b], wfull[q, b], preferred_element_type=f32) for b in range(4))
            conv_v[:, aligned(q * slice_cols, slice_cols)] = total.astype(bf16)
            return carry

        lax.fori_loop(0, xs, one, 0)

    for r in a2a:
        r.wait_recv()
    pass_history()
    for r in params + conv_x:
        r.start()

    slot = lax.broadcasted_iota(i32, (cap, group_rows), 0).astype(f32)

    def ep_copy(c, j):
        s = c * per + j
        return remote(
            outgoing.at[:, aligned(s * cap, cap), :],
            arrived.at[0:2, aligned(s * cap, cap), :],
            ep_send.at[s], ep_recv.at[s], {"ep": partner(c, j, 1)},
        )

    def dispatch(c, carry):
        ranked = ranks[aligned(c * per, per), :]
        pick = jnp.concatenate(
            [jnp.where(ranked[j : j + 1, :] == slot, 1.0, 0.0) for j in range(per)], axis=0
        ).astype(bf16)
        here = aligned(c * chunk, chunk)
        for b in range(2):
            outgoing[b, here, :] = jnp.dot(pick, group[b], preferred_element_type=f32).astype(bf16)

        for j in range(per):
            if j == 0:
                @pl.when(c > 0)
                def _():
                    ep_copy(c, 0).start()
            else:
                ep_copy(c, j).start()
        return carry

    lax.fori_loop(0, zs, dispatch, 0)
    mine = slice(0, cap)
    arrived[0:2, mine, :] = outgoing[:, mine, :]

    def weigh(c, carry):
        ranked = ranks[aligned(c * per, per), :]
        held = held_w[aligned(c * per, per), :]
        block = jnp.concatenate(
            [jnp.where(ranked[j : j + 1, :] == slot, held[j : j + 1, :], 0.0) for j in range(per)], axis=0
        )
        scale[c] = block.T.astype(bf16)
        return carry

    lax.fori_loop(0, zs, weigh, 0)

    def gather_copies(c):
        at = aligned(c * chunk, chunk)
        return [
            remote(arrived.at[1, at, :], arrived.at[2, at, :], gather_send.at[0, c], gather_recv.at[0, c], {"tp": prv}),
            remote(arrived.at[0, at, :], arrived.at[3, at, :], gather_send.at[1, c], gather_recv.at[1, c], {"tp": nxt}),
        ]

    def land(c):
        for j in range(per):
            if j == 0:
                @pl.when(c > 0)
                def _():
                    ep_copy(c, 0).wait_recv()
            else:
                ep_copy(c, j).wait_recv()
        for r in gather_copies(c):
            r.start()

    def return_copies(c):
        at = aligned(c * chunk, chunk)
        low, high = slice(0, half), slice(half, col)

        def one(n, src, dst, where):
            return remote(src, dst, ret_send.at[n, c], ret_recv.at[n, c], {"tp": where})

        return [
            one(0, pieces.at[2, at, low], moe_a.at[at, :], nxt),
            one(1, pieces.at[2, at, high], moe_b.at[at, :], prv),
            one(2, pieces.at[1, at, high], moe_c.at[at, high], nxt),
            one(3, pieces.at[3, at, low], moe_d.at[at, low], prv),
            one(4, moe_u.at[at, :], moe_c.at[at, low], nxt),
            one(5, moe_v.at[at, :], moe_d.at[at, high], prv),
        ]

    def experts(c):
        for r in gather_copies(c):
            r.wait_recv()
        at = aligned(c * chunk, chunk)
        lines = [arrived[k, at, :] for k in range(4)]
        hidden = []
        step = min(256, col)
        for n in range(0, col, step):
            left = sum(jnp.dot(lines[k], gate[k, :, n : n + step], preferred_element_type=f32) for k in range(4))
            right = sum(jnp.dot(lines[k], up[k, :, n : n + step], preferred_element_type=f32) for k in range(4))
            hidden.append((left / (1.0 + jnp.exp(-left)) * right).astype(bf16))
        hid = jnp.concatenate(hidden, axis=1)
        for k in (2, 1, 3, 0):
            pieces[k, at, :] = jnp.dot(hid, down[k], preferred_element_type=f32).astype(bf16)
        for r in return_copies(c)[:4]:
            r.start()

    def middle(c):
        copies = return_copies(c)
        at = aligned(c * chunk, chunk)
        copies[0].wait_recv()
        moe_u[at, :] = (pieces[1, at, :half].astype(f32) + moe_a[at, :].astype(f32)).astype(bf16)
        copies[4].start()
        copies[1].wait_recv()
        moe_v[at, :] = (pieces[3, at, half:].astype(f32) + moe_b[at, :].astype(f32)).astype(bf16)
        copies[5].start()

    def back_copy(c, j):
        s = c * per + j
        at = aligned(s * cap, cap)
        return remote(
            back_out.at[at, :], returned.at[at, :], back_send.at[s], back_recv.at[s],
            {"ep": partner(c, j, -1)},
        )

    def finish(c):
        copies = return_copies(c)
        at = aligned(c * chunk, chunk)
        for n in (2, 3, 4, 5):
            copies[n].wait_recv()
        back_out[at, :] = (
            pieces[0, at, :].astype(f32) + moe_c[at, :].astype(f32) + moe_d[at, :].astype(f32)
        ).astype(bf16)
        for j in range(per):
            if j == 0:
                @pl.when(c > 0)
                def _():
                    back_copy(c, 0).start()
            else:
                back_copy(c, j).start()

    land(0)

    def step(i, carry):
        @pl.when(i < zs - 1)
        def _():
            land(i + 1)

        @pl.when(i == 0)
        def _():
            for load in proj_loads:
                load.wait()
            w_first(1).start()
            w_first(3).start()
            for k in (0, 1, 3):
                convolve(k)
            for load in loads[1:]:
                load.wait()

        @pl.when(i == 1)
        def _():
            w_first(2).start()
            convolve(2)
            lax.fori_loop(0, strips, normalise, 0)

        for n, k in enumerate((1, 3, 2)):
            @pl.when(i == 2 + n)
            def _():
                w_spread(k)

            @pl.when(i == 5 + n)
            def _():
                w_share(k)

        @pl.when(i < zs)
        def _():
            experts(i)

        @pl.when(i == last_step - 1)
        def _():
            multiply(0)

        @pl.when((i >= 1) & (i <= zs))
        def _():
            middle(i - 1)

        @pl.when((i >= 2) & (i < zs + 2))
        def _():
            finish(i - 2)

        return carry

    last_step = max(zs + 1, 9)
    lax.fori_loop(0, last_step, step, 0)
    if cs > 1:
        for k in (1, 3, 2):
            for d in range(xs):
                w_across(k, d).wait_recv()
        multiply(1)
    put = pltpu.make_async_copy(conv_v, conv_out, out_sem)
    put.start()
    if last_step < zs + 2:
        finish(zs - 1)

    returned[mine, :] = back_out[mine, :]
    total = jnp.zeros((group_rows, col), f32)
    for c in range(zs):
        for j in range(per):
            if (c, j) != (0, 0):
                back_copy(c, j).wait_recv()
        total = total + jnp.dot(
            scale[c], returned[c * chunk : (c + 1) * chunk, :], preferred_element_type=f32
        )
    combined[...] = total.astype(bf16)
    last = []
    for k in range(1, 4):
        to = lax.rem(me + k, 4)
        last.append(
            remote(
                combined.at[aligned(to * rows, rows), :], final.at[me],
                fin_send.at[k - 1], fin_recv.at[k - 1], {"tp": to},
            )
        )
    for r in last:
        r.start()
    final[me] = combined[aligned(me * rows, rows), :]
    for r in last:
        r.wait_recv()
    for b in range(4):
        moe_out[:, b * col : (b + 1) * col] = final[b]

    for r in a2a + conv_x + params + [hist] + last:
        r.wait_send()
    for k in range(1, 4):
        w_first(k).wait_send()
        for d in range(1, xs):
            w_along(k, d).wait_send()
        if cs > 1:
            for d in range(xs):
                w_across(k, d).wait_send()

        @pl.when(me == k)
        def _():
            hist_relay(k).wait_send()

    def drain(c, carry):
        for j in range(per):
            if j == 0:
                @pl.when(c > 0)
                def _():
                    ep_copy(c, 0).wait_send()
                    back_copy(c, 0).wait_send()
            else:
                ep_copy(c, j).wait_send()
                back_copy(c, j).wait_send()
        for r in gather_copies(c) + return_copies(c):
            r.wait_send()
        return carry

    lax.fori_loop(0, zs, drain, 0)

    put.wait()


def local(
    conv_input, conv_kernel, norm_gain, norm_shift, conv_proj, moe_input, moe_gain,
    routes, route_weights, gate_proj, up_proj, down_proj, *, dims=DIMS,
):
    zs, xs, cs = dims
    ep_count = zs * xs * cs
    conv_rows, conv_width = conv_input.shape
    rows, width = moe_input.shape
    group_rows = routes.shape[0]
    cap = 16
    slots = ep_count * cap
    col, half = width // 4, width // 8
    span = conv_rows // 4
    hid = gate_proj.shape[2]
    chunk = xs * cs * cap
    per = xs * cs
    vmem, dma = pltpu.VMEM, pltpu.SemaphoreType.DMA
    at_vmem, at_any = pl.BlockSpec(memory_space=pltpu.VMEM), pl.BlockSpec(memory_space=pl.ANY)
    scratch = [
        vmem((32 + conv_rows, conv_width), bf16),
        vmem((4, 32 + span, conv_width), bf16),
        vmem((5, 32, conv_width), bf16),
        vmem((32, conv_width), bf16),
        vmem((4, 32, conv_width), bf16),
        vmem((4, 32, conv_width), f32),
        vmem((2, conv_width), f32),
        vmem((4, 2, conv_width), f32),
        vmem((4, span, conv_width), f32),
        vmem((2, span, 128), f32),
        vmem((4, span, conv_width), bf16),
        vmem((per, 4, conv_width, width // per), bf16),
        vmem((span, width), bf16),
        vmem((4, col, hid), bf16), vmem((4, col, hid), bf16), vmem((4, hid, col), bf16),
        vmem((5, rows, col), bf16),
        vmem((2, group_rows, col), bf16),
        vmem((ep_count, group_rows), f32), vmem((ep_count, group_rows), f32),
        vmem((zs, group_rows, chunk), bf16),
        vmem((2, slots, col), bf16),
        vmem((4, slots, col), bf16),
        vmem((4, slots, col), bf16),
        vmem((slots, half), bf16), vmem((slots, half), bf16),
        vmem((slots, col), bf16), vmem((slots, col), bf16),
        vmem((slots, half), bf16), vmem((slots, half), bf16),
        vmem((slots, col), bf16), vmem((slots, col), bf16),
        vmem((group_rows, col), bf16),
        vmem((4, rows, col), bf16),
        dma((13 + per,)), dma, pltpu.SemaphoreType.REGULAR,
        dma, dma,
        dma((3,)), dma((3,)),
        dma((3,)), dma((3,)),
        dma((3,)), dma((3,)),
        dma((3,)), dma((3,)),
        dma((3,)), dma((3,)),
        dma((3,)), dma((3,)),
        dma((xs - 1, 3)), dma((xs - 1, 3)),
        dma((xs, 3)), dma((xs, 3)),
        dma((ep_count,)), dma((ep_count,)),
        dma((2, zs)), dma((2, zs)),
        dma((6, zs)), dma((6, zs)),
        dma((ep_count,)), dma((ep_count,)),
        dma((3,)), dma((3,)),
    ]
    return pl.pallas_call(
        functools.partial(layer, dims=dims, cap=cap),
        out_shape=(
            jax.ShapeDtypeStruct((span, width), bf16),
            jax.ShapeDtypeStruct((rows, width), bf16),
        ),
        in_specs=[at_vmem] * 7 + [at_any] * 5,
        out_specs=(at_any, at_vmem),
        scratch_shapes=scratch,
        compiler_params=pltpu.CompilerParams(
            collective_id=0, has_side_effects=True, vmem_limit_bytes=60 * 1024 * 1024
        ),
    )(
        moe_input, moe_gain[None, :], routes.T, route_weights.T, conv_kernel, norm_gain[None, :],
        norm_shift[None, :], conv_input, conv_proj, gate_proj, up_proj, down_proj,
    )


def solution(mesh):
    placed = (
        P("ep", "tp"),
        P(None, "tp"),
        P("tp"),
        P("tp"),
        P("tp", None),
        P(("ep", "tp"), None),
        P(),
        P("ep", None),
        P("ep", None),
        P("ep", None, "tp"),
        P("ep", None, "tp"),
        P("ep", "tp", None),
    )
    return jax.shard_map(
        local,
        mesh=mesh,
        in_specs=placed,
        out_specs=(P(("ep", "tp"), None), P(("ep", "tp"), None)),
        check_vma=False,
    )
```

time: 154 us -> 131 us (0.85)
  Pallas kernels: 150 us -> 127 us
    pallas_call x1, Pallas kernels: 150 us -> 127 us  [local(): pl.pallas_call(functools.partial(layer, dims=dims, cap=cap), out_shape=(j...]
where the time goes in v2:
time: 131 us
  Pallas kernels  127 us (97%)
  local copies, waits for them, and re-layouts  3.05 us (2%)
    pallas_call x1, Pallas kernels, local(): pl.pallas_call(functools.partial(layer, dims=dims, cap=cap), out_shape=(j...  127 us
    unnamed x4, local copies, waits for them, and re-layouts  3.05 us

profile of v2, /device:TPU:1, one launch (start us, length us, event | category | flops | bytes accessed | tf_op | source)
XLA Modules:
  0.0 131.2 jit_solution(10899821520897798025)
XLA Ops:
  0.6 127.5 %shard_map.131 = (bf16[256,2048]{1,0:T(8,128)(2,1)}, bf16[64,2048]{1,0:T(8,128)(2,1)}) custom-call(bf16[64,2048]{1,0:T(8,128)(2,1)} %moe_in.1, f32[1,2048]{1,0:T(1,128)} %bitcast.5, s32[2,256]{1,0:T(2,128)} %bitcast.6, f32[2,256]{1,0:T(2,128)} %bitcast.7, bf16[31,512]{1,0:T(8,128)(2,1)} %taps_in.1, f32[1,512]{1,0:T(1,128)} %bitcast.8, f32[1,512]{1,0:T(1,128)} %bitcast.9, ...), custom_call_target="tpu_custom_call" | custom-call | tf_op jit(solution)/shard_map/pallas_call | solution.py:605
  128.1 0.0 copy-start
  128.1 2.3 %copy.16 = bf16[256,2048]{1,0:T(8,128)(2,1)} copy(bf16[256,2048]{1,0:T(8,128)(2,1)} %get-tuple-element.4) | data formatting | bytes 2097152
  130.5 0.0 copy-done
  130.5 0.7 copy.17
Async XLA Ops:
  128.1 2.4 %copy-start = (bf16[64,2048]{1,0:T(8,128)(2,1)S(1)}, bf16[64,2048]{1,0:T(8,128)(2,1)}, u32[]{:S(2)}) copy-start(bf16[64,2048]{1,0:T(8,128)(2,1)} %get-tuple-element.5) | copy-start | bytes 786436

commit v3 on v2

v3 whole, which is shorter than its diff:
```python
import functools

import jax
import jax.numpy as jnp
from jax import lax
from jax.experimental import pallas as pl
from jax.experimental.pallas import tpu as pltpu
from jax.sharding import PartitionSpec as P

MESH = pl.DeviceIdType.MESH
DIMS = (8, 4, 2)
OFFSETS = {8: (0, 3, 5, 4, 2, 6, 1, 7), 4: (0, 2, 1, 3), 2: (0, 1)}
FAR = {8: (1, 4), 4: (1, 2), 2: (2, 2)}
ISSUE = {8: ((0,), (1, 2), (3,), (4, 5), (6, 7)), 4: ((0,), (1,), (2, 3)), 2: ((0,), (1,))}
f32, bf16, i32 = jnp.float32, jnp.bfloat16, jnp.int32


def layer(
    moe_in, moe_gain, routes, weights, taps_in, gain, shift, conv_hbm, proj_hbm, gate_hbm, up_hbm, down_hbm,
    conv_out, moe_out,
    padded, history, taps, affine_src, affine, mixed, xin, act, wfull,
    gate, up, down, own, group, ranks, held_w, scale, outgoing, arrived, pieces,
    moe_a, moe_b, moe_c, moe_d, moe_u, moe_v, back_out, returned, running, combined, final,
    load_sem, ready, hist_send, hist_recv, a2a_send, a2a_recv,
    cx_send, cx_recv, aff_send, aff_recv,
    wy_send, wy_recv, wx_send, wx_recv, wd_send, wd_recv, ep_send, ep_recv,
    gather_send, gather_recv, ret_send, ret_recv, back_send, back_recv, fin_send, fin_recv,
    *, dims, cap,
):
    zs, xs, cs = dims
    ep_count = zs * xs * cs
    per = xs * cs
    chunk = per * cap
    rows, width = moe_in.shape
    col = width // 4
    half = col // 2
    conv_rows = conv_hbm.shape[0]
    conv_width = conv_hbm.shape[1]
    reach = taps_in.shape[0] - 1
    lead = 32
    span = conv_rows // 4
    slice_cols = width // per

    me_ep, me = lax.axis_index("ep"), lax.axis_index("tp")
    core = lax.rem(me_ep, cs)
    mx = lax.rem(lax.div(me_ep, cs), xs)
    mz = lax.div(me_ep, cs * xs)
    nxt, prv = lax.rem(me + 1, 4), lax.rem(me + 3, 4)

    def remote(src, dst, send, recv, where):
        return pltpu.make_async_remote_copy(
            src_ref=src, dst_ref=dst, send_sem=send, recv_sem=recv, device_id=where,
            device_id_type=MESH,
        )

    def received(ref, sem):
        remote(ref, ref, sem, sem, {"tp": lax.rem(me + 1, 4)}).wait_recv()

    def gone(ref, sem):
        remote(ref, ref, sem, sem, {"tp": lax.rem(me + 1, 4)}).wait_send()

    def aligned(start, size):
        return pl.ds(pl.multiple_of(start, size), size)

    offsets = OFFSETS[zs]
    far_from, far_to = FAR[zs]

    def depth(c):
        return offsets[0] + sum(
            (offsets[k] - offsets[k - 1]) * lax.div(c + (zs - k), zs) for k in range(1, zs)
        )

    def place(z, x, c):
        return (z * xs + x) * cs + c

    def partner(c, j, way):
        dx, dc = j // cs, j % cs
        z = lax.rem(mz + way * depth(c) + zs, zs)
        x = lax.rem(mx + way * dx + xs, xs)
        return place(z, x, lax.rem(core + dc, cs))

    barrier = pltpu.get_barrier_semaphore()
    along_z = sorted(range(1, zs), key=lambda d: -min(d, zs - d))
    for d in along_z:
        pl.semaphore_signal(
            barrier, inc=1, device_id={"ep": place(lax.rem(mz + d, zs), mx, core)}, device_id_type=MESH
        )
    for k in (2, 1, 3):
        pl.semaphore_signal(barrier, inc=1, device_id={"tp": lax.rem(me + k, 4)}, device_id_type=MESH)
    for j in range(1, per):
        where = place(mz, lax.rem(mx + j // cs, xs), lax.rem(core + j % cs, cs))
        pl.semaphore_signal(barrier, inc=1, device_id={"ep": where}, device_id_type=MESH)

    loads = [pltpu.make_async_copy(conv_hbm, padded.at[lead:], load_sem.at[0])]
    for q in range(per):
        loads.append(
            pltpu.make_async_copy(
                proj_hbm.at[:, q * slice_cols : (q + 1) * slice_cols], wfull.at[q, me], load_sem.at[1]
            )
        )
    for k in range(4):
        at = lax.rem(me + k, 4) * col
        loads.append(pltpu.make_async_copy(gate_hbm.at[0, aligned(at, col), :], gate.at[k], load_sem.at[2]))
        loads.append(pltpu.make_async_copy(up_hbm.at[0, aligned(at, col), :], up.at[k], load_sem.at[3]))
        loads.append(pltpu.make_async_copy(down_hbm.at[0, :, aligned(at, col)], down.at[k], load_sem.at[4]))
    for load in loads:
        load.start()

    def loaded(ref, n):
        pltpu.make_async_copy(ref, ref, load_sem.at[n]).wait()

    value = moe_in[...].astype(f32)
    normed = (
        value * lax.rsqrt(jnp.mean(value * value, axis=1, keepdims=True) + 1e-06) * moe_gain[...]
    ).astype(bf16)
    for b in range(5):
        own[b] = normed[:, (b % 4) * col : (b % 4 + 1) * col]

    group_rows = routes.shape[1]
    s_at = lax.broadcasted_iota(i32, (ep_count, group_rows), 0)
    per_bits, core_bits = per.bit_length() - 1, cs.bit_length() - 1
    c_at = s_at >> per_bits
    dz = jnp.full_like(c_at, offsets[0])
    for k in range(1, zs):
        dz = jnp.where(c_at == k, offsets[k], dz)
    dx = (s_at & (per - 1)) >> core_bits
    dc = s_at & (cs - 1)
    expert = ((((mz + dz) & (zs - 1)) * xs + ((mx + dx) & (xs - 1))) * cs) + ((core + dc) & (cs - 1))
    first, second = routes[0:1, :] == expert, routes[1:2, :] == expert
    hit = first | second
    before = (
        lax.broadcasted_iota(i32, (group_rows, group_rows), 0)
        < lax.broadcasted_iota(i32, (group_rows, group_rows), 1)
    )
    rank = jnp.dot(
        jnp.where(hit, 1.0, 0.0).astype(bf16), jnp.where(before, 1.0, 0.0).astype(bf16),
        preferred_element_type=f32,
    )
    ranks[...] = jnp.where(hit, rank, -1.0)
    held_w[...] = jnp.where(first, weights[0:1, :], 0.0) + jnp.where(second, weights[1:2, :], 0.0)
    taps[0 : reach + 1, :] = taps_in[...].astype(f32)
    affine_src[0:1, :] = gain[...]
    affine_src[1:2, :] = shift[...]

    lane, strip = 128, min(64, span)

    def conv_strip(i, carry):
        at = aligned(i * strip, strip)
        r0 = pl.multiple_of(i * strip, strip)
        for n in range(0, conv_width, lane):
            x = padded[pl.ds(r0, strip + lead), n : n + lane].astype(f32)
            out = None
            for phase in range(8):
                acc = None
                extra = 8 if phase else 0
                for q in range(lead // 8 + 1):
                    tap = 8 * q + phase - (lead - reach)
                    if tap < 0 or tap > reach:
                        continue
                    term = x[8 * q : 8 * q + strip + extra] * taps[tap : tap + 1, n : n + lane]
                    acc = term if acc is None else acc + term
                if acc is None:
                    continue
                part = acc[phase : phase + strip]
                out = part if out is None else out + part
            mixed[at, n : n + lane] = out.astype(bf16)
        return carry

    strips = conv_rows // strip
    early = strips * 3 // 8
    loaded(padded.at[lead:], 0)
    lax.fori_loop(1, early, conv_strip, 0)

    pl.semaphore_wait(barrier, zs + per + 1)

    slice_id = mx * cs + core

    def w_first(k):
        piece = wfull.at[slice_id, me]
        return remote(piece, piece, wy_send, wy_recv.at[k - 1], {"tp": lax.rem(me + k, 4)})

    half_rows = conv_width // 2

    def w_relay(k):
        to, part = (nxt, slice(0, half_rows)) if k == 1 else (prv, slice(half_rows, conv_width))
        piece = wfull.at[slice_id, lax.rem(me + 4 - k, 4), part]
        return remote(piece, piece, wy_send, wy_recv.at[1], {"tp": to})

    a2a, conv_x, params = [], [], []
    for k in range(1, 4):
        to = lax.rem(me + k, 4)
        a2a.append(
            remote(
                own.at[pl.ds(to, 2)], group.at[:, aligned(me * rows, rows), :],
                a2a_send, a2a_recv, {"tp": to},
            )
        )
        for h in range(2):
            part = span // 2
            conv_x.append(
                remote(
                    mixed.at[aligned(to * span + h * part, part), :], xin.at[me, h * part : (h + 1) * part],
                    cx_send, cx_recv, {"tp": to},
                )
            )
        params.append(remote(affine_src, affine.at[me], aff_send, aff_recv, {"tp": to}))
    for r in a2a:
        r.start()
    loaded(wfull.at[:, 0], 1)
    for k in (1, 3):
        w_first(k).start()
    for d in along_z:
        pl.semaphore_signal(
            ready, inc=1, device_id={"ep": place(lax.rem(mz + d, zs), mx, core)}, device_id_type=MESH
        )
    group[:, aligned(me * rows, rows), :] = own[pl.ds(me, 2)]
    affine[me] = affine_src[...]
    lax.fori_loop(early, strips * 3 // 4, conv_strip, 0)
    pl.semaphore_wait(ready, zs - 1)
    hist = remote(
        padded.at[conv_rows : conv_rows + lead], history, hist_send, hist_recv,
        {"ep": lax.rem(me_ep + 1, ep_count)},
    )
    hist.start()
    lax.fori_loop(strips * 3 // 4, strips, conv_strip, 0)

    def normalise(i, carry):
        at = aligned(i * strip, strip)
        parts = [xin[b, at, :].astype(f32) for b in range(4)]
        one, two = sum(parts), sum(p * p for p in parts)
        center = jnp.sum(one, axis=1, keepdims=True) / width
        square = jnp.sum(two, axis=1, keepdims=True) / width
        inverse = lax.rsqrt(jnp.maximum(square - center * center, 0.0) + 1e-05)
        for b in range(4):
            scaled = (xin[b, at, :].astype(f32) - center) * inverse * affine[b, 0:1, :] + affine[b, 1:2, :]
            act[b, at, :] = (scaled / (1.0 + jnp.exp(-scaled))).astype(bf16)
        return carry

    def w_along(k, d):
        piece = wfull.at[slice_id, lax.rem(me + 4 - k, 4)]
        return remote(
            piece, piece, wx_send, wx_recv.at[k - 1],
            {"ep": place(mz, lax.rem(mx + d, xs), core)},
        )

    def w_across(k, d):
        piece = wfull.at[lax.rem(mx + xs - d, xs) * cs + core, lax.rem(me + 4 - k, 4)]
        return remote(
            piece, piece, wd_send, wd_recv,
            {"ep": place(mz, mx, lax.rem(core + 1, cs))},
        )

    def w_spread(k):
        if k == 2:
            received(wfull.at[0, 0], wy_recv.at[1])
        for d in range(1, xs):
            w_along(k, d).start()
        if cs > 1:
            w_across(k, 0).start()

    def w_share(k):
        received(wfull.at[0 : xs - 1, 0], wx_recv.at[k - 1])
        if cs > 1:
            for d in range(1, xs):
                w_across(k, d).start()

    def multiply(side):
        def one(d, carry):
            q = lax.rem(mx + d, xs) * cs + lax.rem(core + side, cs)
            total = sum(jnp.dot(act[b], wfull[q, b], preferred_element_type=f32) for b in range(4))
            conv_out[:, aligned(q * slice_cols, slice_cols)] = total.astype(bf16)
            return carry

        lax.fori_loop(0, xs, one, 0)

    received(group.at[:, 0 : 3 * rows, :], a2a_recv)
    for r in params:
        r.start()

    slot = lax.broadcasted_iota(i32, (cap, group_rows), 0).astype(f32)

    def ep_copy(c, j):
        s = c * per + j
        blocks = slice(0, 1 if far_from <= c < far_to else 2)
        return remote(
            outgoing.at[blocks, aligned(s * cap, cap), :],
            arrived.at[blocks, aligned(s * cap, cap), :],
            ep_send, ep_recv.at[c], {"ep": partner(c, j, 1)},
        )

    def dispatch(group_of):
        for c in group_of:
            ranked = ranks[c * per : (c + 1) * per, :]
            pick = jnp.concatenate(
                [jnp.where(ranked[j : j + 1, :] == slot, 1.0, 0.0) for j in range(per)], axis=0
            ).astype(bf16)
            for b in range(1 if far_from <= c < far_to else 2):
                outgoing[b, c * chunk : (c + 1) * chunk, :] = jnp.dot(
                    pick, group[b], preferred_element_type=f32
                ).astype(bf16)
        for j in range(per):
            for c in group_of:
                if (c, j) != (0, 0):
                    ep_copy(c, j).start()

    for group_of in ISSUE[zs]:
        dispatch(group_of)
    mine = slice(0, cap)
    arrived[0:2, mine, :] = outgoing[:, mine, :]

    hist.wait_recv()
    padded[0:lead, :] = jnp.where(me_ep == 0, jnp.zeros((lead, conv_width), bf16), history[...])
    lax.fori_loop(0, 1, conv_strip, 0)
    xin[me] = mixed[aligned(me * span, span), :]

    def weigh(c, carry):
        ranked = ranks[aligned(c * per, per), :]
        held = held_w[aligned(c * per, per), :]
        block = jnp.concatenate(
            [jnp.where(ranked[j : j + 1, :] == slot, held[j : j + 1, :], 0.0) for j in range(per)], axis=0
        )
        scale[c] = block.T.astype(bf16)
        return carry

    lax.fori_loop(0, zs, weigh, 0)

    def is_far(c):
        return (c >= far_from) & (c < far_to)

    def gather_copy(n, c):
        at = aligned(c * chunk, chunk)
        low, high = slice(0, half), slice(half, col)
        src, dst, where = [
            (arrived.at[1, at, :], arrived.at[2, at, :], prv),
            (arrived.at[0, at, :], arrived.at[3, at, :], nxt),
            (arrived.at[0, at, :], arrived.at[1, at, :], prv),
            (arrived.at[1, at, low], arrived.at[2, at, low], prv),
            (arrived.at[3, at, high], arrived.at[2, at, high], nxt),
        ][n]
        sem = (0, 1, 0, 2, 2)[n]
        return remote(src, dst, gather_send.at[sem], gather_recv.at[sem, c], {"tp": where})

    def land(c):
        at = aligned(c * chunk, chunk)

        @pl.when(c == 0)
        def _():
            received(arrived.at[0:2, 0 : chunk - cap, :], ep_recv.at[c])

        @pl.when((c > 0) & jnp.logical_not(is_far(c)))
        def _():
            received(arrived.at[0:2, at, :], ep_recv.at[c])

        @pl.when(is_far(c))
        def _():
            received(arrived.at[0, at, :], ep_recv.at[c])
            gather_copy(2, c).start()

        @pl.when(jnp.logical_not(is_far(c)))
        def _():
            gather_copy(0, c).start()

        gather_copy(1, c).start()

    def relay(c):
        at = aligned(c * chunk, chunk)
        received(arrived.at[1, at, :], gather_recv.at[0, c])
        gather_copy(3, c).start()
        received(arrived.at[3, at, :], gather_recv.at[1, c])
        gather_copy(4, c).start()

    def return_copies(c):
        at = aligned(c * chunk, chunk)
        low, high = slice(0, half), slice(half, col)

        def one(n, src, dst, where):
            return remote(src, dst, ret_send.at[n], ret_recv.at[n, c], {"tp": where})

        return [
            one(0, pieces.at[2, at, low], moe_a.at[at, :], nxt),
            one(1, pieces.at[2, at, high], moe_b.at[at, :], prv),
            one(2, pieces.at[1, at, high], moe_c.at[at, high], nxt),
            one(3, pieces.at[3, at, low], moe_d.at[at, low], prv),
            one(2, moe_u.at[at, :], moe_c.at[at, low], nxt),
            one(3, moe_v.at[at, :], moe_d.at[at, high], prv),
        ]

    def experts(c):
        at = aligned(c * chunk, chunk)

        @pl.when(is_far(c))
        def _():
            received(arrived.at[2, at, :], gather_recv.at[2, c])

        @pl.when(jnp.logical_not(is_far(c)))
        def _():
            received(arrived.at[2, at, :], gather_recv.at[0, c])
            received(arrived.at[3, at, :], gather_recv.at[1, c])

        lines = [arrived[k, at, :] for k in range(4)]
        hidden = []
        step = min(256, col)
        for n in range(0, col, step):
            left = sum(jnp.dot(lines[k], gate[k, :, n : n + step], preferred_element_type=f32) for k in range(4))
            right = sum(jnp.dot(lines[k], up[k, :, n : n + step], preferred_element_type=f32) for k in range(4))
            hidden.append((left / (1.0 + jnp.exp(-left)) * right).astype(bf16))
        hid = jnp.concatenate(hidden, axis=1)
        for k in (2, 1, 3, 0):
            pieces[k, at, :] = jnp.dot(hid, down[k], preferred_element_type=f32).astype(bf16)
        for r in return_copies(c)[:4]:
            r.start()

    def middle(c):
        copies = return_copies(c)
        at = aligned(c * chunk, chunk)
        copies[0].wait_recv()
        moe_u[at, :] = (pieces[1, at, :half].astype(f32) + moe_a[at, :].astype(f32)).astype(bf16)
        copies[4].start()
        copies[1].wait_recv()
        moe_v[at, :] = (pieces[3, at, half:].astype(f32) + moe_b[at, :].astype(f32)).astype(bf16)
        copies[5].start()

    def back_copy(c, j):
        s = c * per + j
        at = aligned(s * cap, cap)
        return remote(
            back_out.at[at, :], returned.at[at, :], back_send, back_recv.at[c],
            {"ep": partner(c, j, -1)},
        )

    def finish(c):
        at = aligned(c * chunk, chunk)
        received(moe_c.at[at, :], ret_recv.at[2, c])
        received(moe_d.at[at, :], ret_recv.at[3, c])
        back_out[at, :] = (
            pieces[0, at, :].astype(f32) + moe_c[at, :].astype(f32) + moe_d[at, :].astype(f32)
        ).astype(bf16)
        for j in range(per):
            if j == 0:
                @pl.when(c > 0)
                def _():
                    back_copy(c, 0).start()
            else:
                back_copy(c, j).start()

    for k in (1, 3):
        received(wfull.at[0, 0], wy_recv.at[k - 1])
        w_relay(k).start()
    land(0)

    def step(i, carry):
        @pl.when((i >= 3) & (i + 2 < zs))
        def _():
            land(i + 2)

        for n in (1, 2):
            if far_from <= n < far_to:
                @pl.when(i == 1)
                def _():
                    relay(n)

        @pl.when(i == 0)
        def _():
            loaded(gate, 2)
            loaded(up, 3)
            loaded(down, 4)

        experts(i)

        for n in range(max(far_from, 3), far_to):
            @pl.when(i == n - 1)
            def _():
                relay(n)

        @pl.when(i >= 1)
        def _():
            middle(i - 1)

        @pl.when(i >= 2)
        def _():
            finish(i - 2)

        for n, k in enumerate((1, 3, 2)):
            @pl.when(i == spread_at[n])
            def _():
                w_spread(k)

            @pl.when(i == share_at[n])
            def _():
                w_share(k)

        for n, at_end in ((1, 0), (2, 0), (3, 1), (4, 2)):
            if n < zs:
                @pl.when(i == at_end)
                def _():
                    land(n)

        return carry

    spread_at = [min(n, zs - 1) for n in (0, 1, 2)]
    share_at = [min(n, zs - 1) for n in (5, 6, 7)]
    lax.fori_loop(0, zs, step, 0)
    middle(zs - 1)
    finish(zs - 2)
    for r in conv_x:
        r.start()
    finish(zs - 1)

    returned[mine, :] = back_out[mine, :]
    def combine(c):
        here = slice(c * chunk + (0 if c else cap), (c + 1) * chunk)
        received(returned.at[here, :], back_recv.at[c])
        return jnp.dot(scale[c], returned[c * chunk : (c + 1) * chunk, :], preferred_element_type=f32)

    total = combine(0)
    for c in range(1, zs - 1):
        total = total + combine(c)
    running[...] = total
    total = running[...] + combine(zs - 1)
    combined[...] = total.astype(bf16)
    last = []
    for k in range(1, 4):
        to = lax.rem(me + k, 4)
        last.append(
            remote(
                combined.at[aligned(to * rows, rows), :], final.at[me],
                fin_send, fin_recv, {"tp": to},
            )
        )
    for r in last:
        r.start()
    final[me] = combined[aligned(me * rows, rows), :]
    received(affine.at[0:3], aff_recv)
    received(xin.at[0:3], cx_recv)
    lax.fori_loop(0, span // strip, normalise, 0)
    multiply(0)
    if cs > 1:
        received(wfull.at[0:xs, 0:3], wd_recv)
        multiply(1)
    received(final.at[0:3], fin_recv)
    for b in range(4):
        moe_out[:, b * col : (b + 1) * col] = final[b]

    gone(own.at[0:6], a2a_send)
    gone(xin.at[0:3], cx_send)
    gone(affine.at[0:3], aff_send)
    hist.wait_send()
    gone(wfull.at[0:3, 0], wy_send)
    gone(wfull.at[0 : xs - 1, 0:3], wx_send)
    if cs > 1:
        gone(wfull.at[0:xs, 0:3], wd_send)
    sent = (2 * (zs - far_to + far_from) + far_to - far_from) * chunk // 2 - cap
    gone(outgoing.at[:, 0:sent, :], ep_send)
    gone(arrived.at[0], gather_send.at[0])
    gone(arrived.at[0], gather_send.at[1])
    if far_to > far_from:
        gone(arrived.at[0, 0 : (far_to - far_from) * chunk], gather_send.at[2])
    gone(moe_a, ret_send.at[0])
    gone(moe_b, ret_send.at[1])
    gone(moe_c, ret_send.at[2])
    gone(moe_d, ret_send.at[3])
    gone(back_out.at[cap:, :], back_send)
    gone(final.at[0:3], fin_send)


def local(
    conv_input, conv_kernel, norm_gain, norm_shift, conv_proj, moe_input, moe_gain,
    routes, route_weights, gate_proj, up_proj, down_proj, *, dims=DIMS,
):
    zs, xs, cs = dims
    ep_count = zs * xs * cs
    conv_rows, conv_width = conv_input.shape
    rows, width = moe_input.shape
    group_rows = routes.shape[0]
    cap = 16
    slots = ep_count * cap
    col, half = width // 4, width // 8
    span = conv_rows // 4
    hid = gate_proj.shape[2]
    chunk = xs * cs * cap
    per = xs * cs
    vmem, dma = pltpu.VMEM, pltpu.SemaphoreType.DMA
    at_vmem, at_hbm = pl.BlockSpec(memory_space=pltpu.VMEM), pl.BlockSpec(memory_space=pltpu.HBM)
    scratch = [
        vmem((32 + conv_rows, conv_width), bf16),
        vmem((32, conv_width), bf16),
        vmem((32, conv_width), f32),
        vmem((2, conv_width), f32),
        vmem((4, 2, conv_width), f32),
        vmem((conv_rows, conv_width), bf16),
        vmem((4, span, conv_width), bf16),
        vmem((4, span, conv_width), bf16),
        vmem((per, 4, conv_width, width // per), bf16),
        vmem((4, col, hid), bf16), vmem((4, col, hid), bf16), vmem((4, hid, col), bf16),
        vmem((6, rows, col), bf16),
        vmem((2, group_rows, col), bf16),
        vmem((ep_count, group_rows), f32), vmem((ep_count, group_rows), f32),
        vmem((zs, group_rows, chunk), bf16),
        vmem((2, slots, col), bf16),
        vmem((4, slots, col), bf16),
        vmem((4, slots, col), bf16),
        vmem((slots, half), bf16), vmem((slots, half), bf16),
        vmem((slots, col), bf16), vmem((slots, col), bf16),
        vmem((slots, half), bf16), vmem((slots, half), bf16),
        vmem((slots, col), bf16), vmem((slots, col), bf16),
        vmem((group_rows, col), f32),
        vmem((group_rows, col), bf16),
        vmem((4, rows, col), bf16),
        dma((5,)), pltpu.SemaphoreType.REGULAR,
        dma, dma,
        dma, dma,
        dma, dma,
        dma, dma,
        dma, dma((3,)),
        dma, dma((3,)),
        dma, dma,
        dma, dma((zs,)),
        dma((3,)), dma((3, zs)),
        dma((4,)), dma((4, zs)),
        dma, dma((zs,)),
        dma, dma,
    ]
    return pl.pallas_call(
        functools.partial(layer, dims=dims, cap=cap),
        out_shape=(
            jax.ShapeDtypeStruct((span, width), bf16),
            jax.ShapeDtypeStruct((rows, width), bf16),
        ),
        in_specs=[at_vmem] * 7 + [at_hbm] * 5,
        out_specs=(at_vmem, at_vmem),
        scratch_shapes=scratch,
        compiler_params=pltpu.CompilerParams(
            collective_id=0, has_side_effects=True, vmem_limit_bytes=60 * 1024 * 1024
        ),
    )(
        moe_input, moe_gain[None, :], routes.T, route_weights.T, conv_kernel, norm_gain[None, :],
        norm_shift[None, :], conv_input, conv_proj, gate_proj, up_proj, down_proj,
    )


def solution(mesh):
    placed = (
        P("ep", "tp"),
        P(None, "tp"),
        P("tp"),
        P("tp"),
        P("tp", None),
        P(("ep", "tp"), None),
        P(),
        P("ep", None),
        P("ep", None),
        P("ep", None, "tp"),
        P("ep", None, "tp"),
        P("ep", "tp", None),
    )
    return jax.shard_map(
        local,
        mesh=mesh,
        in_specs=placed,
        out_specs=(P(("ep", "tp"), None), P(("ep", "tp"), None)),
        check_vma=False,
    )
```

time: 131 us -> 117 us (0.89); the launches traced: 131 us -> 115 us
  Pallas kernels: 127 us -> 111 us
    pallas_call x1, Pallas kernels: 127 us -> 111 us  [local(): pl.pallas_call(functools.partial(layer, dims=dims, cap=cap), out_shape=(j...]
where the time goes in v3:
time: 117 us; the launch traced here: 115 us
  Pallas kernels  111 us (95%)
  local copies, waits for them, and re-layouts  3.05 us (3%)
    pallas_call x1, Pallas kernels, local(): pl.pallas_call(functools.partial(layer, dims=dims, cap=cap), out_shape=(j...  111 us
    unnamed x4, local copies, waits for them, and re-layouts  3.05 us

profile of v3, /device:TPU:1, one launch (start us, length us, event | category | flops | bytes accessed | tf_op | source)
XLA Modules:
  0.0 115.1 jit_solution(14781212899190114185)
XLA Ops:
  0.6 111.4 %shard_map.131 = (bf16[256,2048]{1,0:T(8,128)(2,1)}, bf16[64,2048]{1,0:T(8,128)(2,1)}) custom-call(bf16[64,2048]{1,0:T(8,128)(2,1)} %moe_in.1, f32[1,2048]{1,0:T(1,128)} %bitcast.5, s32[2,256]{1,0:T(2,128)} %bitcast.6, f32[2,256]{1,0:T(2,128)} %bitcast.7, bf16[31,512]{1,0:T(8,128)(2,1)} %taps_in.1, f32[1,512]{1,0:T(1,128)} %bitcast.8, f32[1,512]{1,0:T(1,128)} %bitcast.9, ...), custom_call_target="tpu_custom_call" | custom-call | tf_op jit(solution)/shard_map/pallas_call | solution.py:623
  112.1 0.0 copy-start
  112.1 2.3 %copy.16 = bf16[256,2048]{1,0:T(8,128)(2,1)} copy(bf16[256,2048]{1,0:T(8,128)(2,1)} %get-tuple-element.4) | data formatting | bytes 2097152
  114.4 0.0 copy-done
  114.4 0.7 copy.17
Async XLA Ops:
  112.1 2.4 %copy-start = (bf16[64,2048]{1,0:T(8,128)(2,1)S(1)}, bf16[64,2048]{1,0:T(8,128)(2,1)}, u32[]{:S(2)}) copy-start(bf16[64,2048]{1,0:T(8,128)(2,1)} %get-tuple-element.5) | copy-start | bytes 786436

commit v4 on v3

--- a/solution.py
+++ b/solution.py
@@ -18,12 +18,12 @@
 def layer(
     moe_in, moe_gain, routes, weights, taps_in, gain, shift, conv_hbm, proj_hbm, gate_hbm, up_hbm, down_hbm,
     conv_out, moe_out,
-    padded, history, taps, affine_src, affine, mixed, xin, act, wfull,
+    padded, history, taps, mixed, sums, stats, stats_in, columns, active, xin, conv_sum, wfull,
     gate, up, down, own, group, ranks, held_w, scale, outgoing, arrived, pieces,
     moe_a, moe_b, moe_c, moe_d, moe_u, moe_v, back_out, returned, running, combined, final,
     load_sem, ready, hist_send, hist_recv, a2a_send, a2a_recv,
-    cx_send, cx_recv, aff_send, aff_recv,
-    wy_send, wy_recv, wx_send, wx_recv, wd_send, wd_recv, ep_send, ep_recv,
+    cx_send, cx_recv, stat_send, stat_recv,
+    wy_send, wy_recv, wz_send, wz_recv, wx_send, wx_recv, wd_send, wd_recv, ep_send, ep_recv,
     gather_send, gather_recv, ret_send, ret_recv, back_send, back_recv, fin_send, fin_recv,
     *, dims, cap,
 ):
@@ -45,7 +45,7 @@
     core = lax.rem(me_ep, cs)
     mx = lax.rem(lax.div(me_ep, cs), xs)
     mz = lax.div(me_ep, cs * xs)
-    nxt, prv = lax.rem(me + 1, 4), lax.rem(me + 3, 4)
+    nxt, opp, prv = lax.rem(me + 1, 4), lax.rem(me + 2, 4), lax.rem(me + 3, 4)
 
     def remote(src, dst, send, recv, where):
         return pltpu.make_async_remote_copy(
@@ -139,54 +139,69 @@
     ranks[...] = jnp.where(hit, rank, -1.0)
     held_w[...] = jnp.where(first, weights[0:1, :], 0.0) + jnp.where(second, weights[1:2, :], 0.0)
     taps[0 : reach + 1, :] = taps_in[...].astype(f32)
-    affine_src[0:1, :] = gain[...]
-    affine_src[1:2, :] = shift[...]
-
-    lane, strip = 128, min(64, span)
-
-    def conv_strip(i, carry):
-        at = aligned(i * strip, strip)
-        r0 = pl.multiple_of(i * strip, strip)
-        for n in range(0, conv_width, lane):
-            x = padded[pl.ds(r0, strip + lead), n : n + lane].astype(f32)
-            out = None
-            for phase in range(8):
-                acc = None
-                extra = 8 if phase else 0
-                for q in range(lead // 8 + 1):
-                    tap = 8 * q + phase - (lead - reach)
-                    if tap < 0 or tap > reach:
+
+    tile = span // 2
+    tiles = conv_rows // tile
+    lane, strip = 128, min(64, tile)
+
+    def conv_tile(i, carry):
+        for h in range(tile // strip):
+            r0 = pl.multiple_of(i * tile + h * strip, strip)
+            one = jnp.zeros((strip, lane), f32)
+            two = jnp.zeros((strip, lane), f32)
+            for n in range(0, conv_width, lane):
+                x = padded[pl.ds(r0, strip + lead), n : n + lane].astype(f32)
+                out = None
+                for phase in range(8):
+                    acc = None
+                    extra = 8 if phase else 0
+                    for q in range(lead // 8 + 1):
+                        tap = 8 * q + phase - (lead - reach)
+                        if tap < 0 or tap > reach:
+                            continue
+                        term = x[8 * q : 8 * q + strip + extra] * taps[tap : tap + 1, n : n + lane]
+                        acc = term if acc is None else acc + term
+                    if acc is None:
                         continue
-                    term = x[8 * q : 8 * q + strip + extra] * taps[tap : tap + 1, n : n + lane]
-                    acc = term if acc is None else acc + term
-                if acc is None:
-                    continue
-                part = acc[phase : phase + strip]
-                out = part if out is None else out + part
-            mixed[at, n : n + lane] = out.astype(bf16)
+                    part = acc[phase : phase + strip]
+                    out = part if out is None else out + part
+                mixed[pl.ds(r0, strip), n : n + lane] = out
+                one = one + out
+                two = two + out * out
+            sums[0, h * strip : (h + 1) * strip, :] = one
+            sums[1, h * strip : (h + 1) * strip, :] = two
+        for m in range(2):
+            stats[m, pl.ds(i, 1), :] = jnp.sum(sums[m].T, axis=0, keepdims=True)
         return carry
 
-    strips = conv_rows // strip
-    early = strips * 3 // 8
+    early = tiles * 3 // 8
     loaded(padded.at[lead:], 0)
-    lax.fori_loop(1, early, conv_strip, 0)
+    lax.fori_loop(1, early, conv_tile, 0)
 
     pl.semaphore_wait(barrier, zs + per + 1)
 
     slice_id = mx * cs + core
 
+    own_rows = conv_width // 2
+    parity = lax.rem(mz, 2)
+    half_rows = own_rows // 2
+
     def w_first(k):
-        piece = wfull.at[slice_id, me]
+        piece = wfull.at[slice_id, me, aligned(parity * own_rows, own_rows)]
         return remote(piece, piece, wy_send, wy_recv.at[k - 1], {"tp": lax.rem(me + k, 4)})
 
-    half_rows = conv_width // 2
-
     def w_relay(k):
-        to, part = (nxt, slice(0, half_rows)) if k == 1 else (prv, slice(half_rows, conv_width))
-        piece = wfull.at[slice_id, lax.rem(me + 4 - k, 4), part]
+        to, part = (nxt, 0) if k == 1 else (prv, half_rows)
+        rows_at = aligned(parity * own_rows + part, half_rows)
+        piece = wfull.at[slice_id, lax.rem(me + 4 - k, 4), rows_at]
         return remote(piece, piece, wy_send, wy_recv.at[1], {"tp": to})
 
-    a2a, conv_x, params = [], [], []
+    def w_pair(k):
+        piece = wfull.at[slice_id, lax.rem(me + 4 - k, 4), aligned(parity * own_rows, own_rows)]
+        where = place(mz + 1 - 2 * parity, mx, core)
+        return remote(piece, piece, wz_send, wz_recv.at[k - 1], {"ep": where})
+
+    a2a, conv_x, moments = [], [], []
     for k in range(1, 4):
         to = lax.rem(me + k, 4)
         a2a.append(
@@ -195,51 +210,59 @@
                 a2a_send, a2a_recv, {"tp": to},
             )
         )
-        for h in range(2):
-            part = span // 2
-            conv_x.append(
-                remote(
-                    mixed.at[aligned(to * span + h * part, part), :], xin.at[me, h * part : (h + 1) * part],
-                    cx_send, cx_recv, {"tp": to},
-                )
+        conv_x.append(
+            remote(
+                active.at[aligned(to * span, span), :], xin.at[me], cx_send, cx_recv.at[k - 1], {"tp": to},
             )
-        params.append(remote(affine_src, affine.at[me], aff_send, aff_recv, {"tp": to}))
+        )
+        moments.append(remote(stats, stats_in.at[k - 1], stat_send, stat_recv, {"tp": to}))
     for r in a2a:
         r.start()
-    loaded(wfull.at[:, 0], 1)
-    for k in (1, 3):
-        w_first(k).start()
     for d in along_z:
         pl.semaphore_signal(
             ready, inc=1, device_id={"ep": place(lax.rem(mz + d, zs), mx, core)}, device_id_type=MESH
         )
     group[:, aligned(me * rows, rows), :] = own[pl.ds(me, 2)]
-    affine[me] = affine_src[...]
-    lax.fori_loop(early, strips * 3 // 4, conv_strip, 0)
+    lax.fori_loop(early, tiles * 3 // 4, conv_tile, 0)
     pl.semaphore_wait(ready, zs - 1)
     hist = remote(
         padded.at[conv_rows : conv_rows + lead], history, hist_send, hist_recv,
         {"ep": lax.rem(me_ep + 1, ep_count)},
     )
     hist.start()
-    lax.fori_loop(strips * 3 // 4, strips, conv_strip, 0)
-
-    def normalise(i, carry):
-        at = aligned(i * strip, strip)
-        parts = [xin[b, at, :].astype(f32) for b in range(4)]
-        one, two = sum(parts), sum(p * p for p in parts)
-        center = jnp.sum(one, axis=1, keepdims=True) / width
-        square = jnp.sum(two, axis=1, keepdims=True) / width
-        inverse = lax.rsqrt(jnp.maximum(square - center * center, 0.0) + 1e-05)
-        for b in range(4):
-            scaled = (xin[b, at, :].astype(f32) - center) * inverse * affine[b, 0:1, :] + affine[b, 1:2, :]
-            act[b, at, :] = (scaled / (1.0 + jnp.exp(-scaled))).astype(bf16)
+    lax.fori_loop(tiles * 3 // 4, tiles, conv_tile, 0)
+
+    def center_and_scale():
+        received(stats_in, stat_recv)
+        total = (stats[...] + stats_in[0] + stats_in[1] + stats_in[2]) / width
+        center = total[0]
+        spread = jnp.maximum(total[1] - center * center, 0.0)
+        inverse = lax.rsqrt(spread + 1e-05)
+        for i in range(tiles):
+            both = jnp.concatenate([center[i : i + 1], inverse[i : i + 1]] + [center[i : i + 1]] * 6, axis=0)
+            columns[i * tile : (i + 1) * tile, :] = both.T
+
+    def activate(i, carry):
+        view = aligned(i * strip, strip)
+        stat = columns[view, :]
+        scaled = (mixed[view, :] - stat[:, 0:1]) * stat[:, 1:2] * gain[...] + shift[...]
+        active[view, :] = (scaled / (1.0 + jnp.exp(-scaled))).astype(bf16)
         return carry
+
+    ends = (1, xs - 1) if xs > 2 else (1,)
 
     def w_along(k, d):
         piece = wfull.at[slice_id, lax.rem(me + 4 - k, 4)]
         return remote(
-            piece, piece, wx_send, wx_recv.at[k - 1],
+            piece, piece, wx_send, wx_recv.at[0 if d == 1 else 1, k - 1],
+            {"ep": place(mz, lax.rem(mx + d, xs), core)},
+        )
+
+    def w_onward(k, d):
+        at = 0 if d == 1 else own_rows
+        piece = wfull.at[lax.rem(mx + xs - d, xs) * cs + core, lax.rem(me + 4 - k, 4), at : at + own_rows]
+        return remote(
+            piece, piece, wx_send, wx_recv.at[2, k - 1],
             {"ep": place(mz, lax.rem(mx + d, xs), core)},
         )
 
@@ -251,31 +274,42 @@
         )
 
     def w_spread(k):
-        if k == 2:
-            received(wfull.at[0, 0], wy_recv.at[1])
-        for d in range(1, xs):
+        received(wfull.at[0, 0, 0:own_rows], wz_recv.at[k - 1])
+        for d in ends:
             w_along(k, d).start()
         if cs > 1:
             w_across(k, 0).start()
 
+    def w_hop(k):
+        for n, d in enumerate(ends):
+            received(wfull.at[0, 0], wx_recv.at[n, k - 1])
+            if xs > 2:
+                w_onward(k, d).start()
+            if cs > 1:
+                w_across(k, d).start()
+
     def w_share(k):
-        received(wfull.at[0 : xs - 1, 0], wx_recv.at[k - 1])
-        if cs > 1:
-            for d in range(1, xs):
-                w_across(k, d).start()
-
-    def multiply(side):
-        def one(d, carry):
-            q = lax.rem(mx + d, xs) * cs + lax.rem(core + side, cs)
-            total = sum(jnp.dot(act[b], wfull[q, b], preferred_element_type=f32) for b in range(4))
-            conv_out[:, aligned(q * slice_cols, slice_cols)] = total.astype(bf16)
-            return carry
-
-        lax.fori_loop(0, xs, one, 0)
+        if xs > 2:
+            received(wfull.at[0, 0], wx_recv.at[2, k - 1])
+            if cs > 1:
+                w_across(k, 2).start()
+
+    def multiply(q, carry):
+        total = sum(
+            jnp.dot(xin[b], wfull[q, b], preferred_element_type=f32) for b in (me, prv, nxt)
+        )
+        conv_sum[q] = total
+        return carry
+
+    def multiply_last(q, carry):
+        total = conv_sum[q] + jnp.dot(xin[opp], wfull[q, opp], preferred_element_type=f32)
+        conv_out[:, aligned(q * slice_cols, slice_cols)] = total.astype(bf16)
+        return carry
 
     received(group.at[:, 0 : 3 * rows, :], a2a_recv)
-    for r in params:
-        r.start()
+    loaded(wfull.at[:, 0], 1)
+    for k in (1, 3):
+        w_first(k).start()
 
     slot = lax.broadcasted_iota(i32, (cap, group_rows), 0).astype(f32)
 
@@ -310,8 +344,9 @@
 
     hist.wait_recv()
     padded[0:lead, :] = jnp.where(me_ep == 0, jnp.zeros((lead, conv_width), bf16), history[...])
-    lax.fori_loop(0, 1, conv_strip, 0)
-    xin[me] = mixed[aligned(me * span, span), :]
+    lax.fori_loop(0, 1, conv_tile, 0)
+    for r in moments:
+        r.start()
 
     def weigh(c, carry):
         ranked = ranks[aligned(c * per, per), :]
@@ -443,10 +478,11 @@
             else:
                 back_copy(c, j).start()
 
+    land(0)
     for k in (1, 3):
-        received(wfull.at[0, 0], wy_recv.at[k - 1])
+        received(wfull.at[0, 0, 0:own_rows], wy_recv.at[k - 1])
         w_relay(k).start()
-    land(0)
+        w_pair(k).start()
 
     def step(i, carry):
         @pl.when((i >= 3) & (i + 2 < zs))
@@ -480,14 +516,22 @@
         def _():
             finish(i - 2)
 
+        @pl.when(i == 0)
+        def _():
+            center_and_scale()
+            lax.fori_loop(0, conv_rows // strip, activate, 0)
+            xin[me] = active[aligned(me * span, span), :]
+            received(wfull.at[0, 0, 0:own_rows], wy_recv.at[1])
+            w_pair(2).start()
+
         for n, k in enumerate((1, 3, 2)):
             @pl.when(i == spread_at[n])
             def _():
                 w_spread(k)
 
-            @pl.when(i == share_at[n])
+            @pl.when(i == hop_at[n])
             def _():
-                w_share(k)
+                w_hop(k)
 
         for n, at_end in ((1, 0), (2, 0), (3, 1), (4, 2)):
             if n < zs:
@@ -497,14 +541,17 @@
 
         return carry
 
-    spread_at = [min(n, zs - 1) for n in (0, 1, 2)]
-    share_at = [min(n, zs - 1) for n in (5, 6, 7)]
+    spread_at = [min(n, zs - 1) for n in (2, 2, 3)]
+    hop_at = [min(n, zs - 1) for n in (4, 5, 6)]
     lax.fori_loop(0, zs, step, 0)
     middle(zs - 1)
+    conv_x[0].start()
+    conv_x[2].start()
     finish(zs - 2)
-    for r in conv_x:
-        r.start()
     finish(zs - 1)
+    conv_x[1].start()
+    for k in (1, 3, 2):
+        w_share(k)
 
     returned[mine, :] = back_out[mine, :]
     def combine(c):
@@ -530,22 +577,23 @@
     for r in last:
         r.start()
     final[me] = combined[aligned(me * rows, rows), :]
-    received(affine.at[0:3], aff_recv)
-    received(xin.at[0:3], cx_recv)
-    lax.fori_loop(0, span // strip, normalise, 0)
-    multiply(0)
+    received(xin.at[0], cx_recv.at[0])
+    received(xin.at[0], cx_recv.at[2])
     if cs > 1:
         received(wfull.at[0:xs, 0:3], wd_recv)
-        multiply(1)
+    lax.fori_loop(0, per, multiply, 0)
+    received(xin.at[0], cx_recv.at[1])
+    lax.fori_loop(0, per, multiply_last, 0)
     received(final.at[0:3], fin_recv)
     for b in range(4):
         moe_out[:, b * col : (b + 1) * col] = final[b]
 
     gone(own.at[0:6], a2a_send)
     gone(xin.at[0:3], cx_send)
-    gone(affine.at[0:3], aff_send)
+    gone(stats_in, stat_send)
     hist.wait_send()
-    gone(wfull.at[0:3, 0], wy_send)
+    gone(wfull.at[0, 0:3, 0:own_rows], wy_send)
+    gone(wfull.at[0, 0:3, 0:own_rows], wz_send)
     gone(wfull.at[0 : xs - 1, 0:3], wx_send)
     if cs > 1:
         gone(wfull.at[0:xs, 0:3], wd_send)
@@ -585,11 +633,14 @@
         vmem((32 + conv_rows, conv_width), bf16),
         vmem((32, conv_width), bf16),
         vmem((32, conv_width), f32),
-        vmem((2, conv_width), f32),
-        vmem((4, 2, conv_width), f32),
+        vmem((conv_rows, conv_width), f32),
+        vmem((2, span // 2, 128), f32),
+        vmem((2, 8, span // 2), f32),
+        vmem((3, 2, 8, span // 2), f32),
+        vmem((conv_rows, 8), f32),
         vmem((conv_rows, conv_width), bf16),
         vmem((4, span, conv_width), bf16),
-        vmem((4, span, conv_width), bf16),
+        vmem((per, span, width // per), f32),
         vmem((per, 4, conv_width, width // per), bf16),
         vmem((4, col, hid), bf16), vmem((4, col, hid), bf16), vmem((4, hid, col), bf16),
         vmem((6, rows, col), bf16),
@@ -609,10 +660,11 @@
         dma((5,)), pltpu.SemaphoreType.REGULAR,
         dma, dma,
         dma, dma,
-        dma, dma,
+        dma, dma((3,)),
         dma, dma,
         dma, dma((3,)),
         dma, dma((3,)),
+        dma, dma((3, 3)),
         dma, dma,
         dma, dma((zs,)),
         dma((3,)), dma((3, zs)),

time: 117 us -> 114 us (0.974); the launches traced: 115 us -> 114 us
  no operation moved by 1% of the time
where the time goes in v4:
time: 114 us
  Pallas kernels  110 us (96%)
  local copies, waits for them, and re-layouts  3.05 us (3%)
    pallas_call x1, Pallas kernels, local(): pl.pallas_call(functools.partial(layer, dims=dims, cap=cap), out_shape=(j...  110 us
    unnamed x4, local copies, waits for them, and re-layouts  3.05 us

profile of v4, /device:TPU:1, one launch (start us, length us, event | category | flops | bytes accessed | tf_op | source)
XLA Modules:
  0.0 114.0 jit_solution(11305517197991379140)
XLA Ops:
  0.6 110.3 %shard_map.131 = (bf16[256,2048]{1,0:T(8,128)(2,1)}, bf16[64,2048]{1,0:T(8,128)(2,1)}) custom-call(bf16[64,2048]{1,0:T(8,128)(2,1)} %moe_in.1, f32[1,2048]{1,0:T(1,128)} %bitcast.5, s32[2,256]{1,0:T(2,128)} %bitcast.6, f32[2,256]{1,0:T(2,128)} %bitcast.7, bf16[31,512]{1,0:T(8,128)(2,1)} %taps_in.1, f32[1,512]{1,0:T(1,128)} %bitcast.8, f32[1,512]{1,0:T(1,128)} %bitcast.9, ...), custom_call_target="tpu_custom_call" | custom-call | tf_op jit(solution)/shard_map/pallas_call | solution.py:675
  110.9 0.0 copy-start
  110.9 2.3 %copy.16 = bf16[256,2048]{1,0:T(8,128)(2,1)} copy(bf16[256,2048]{1,0:T(8,128)(2,1)} %get-tuple-element.4) | data formatting | bytes 2097152
  113.3 0.0 copy-done
  113.3 0.7 copy.17
Async XLA Ops:
  110.9 2.4 %copy-start = (bf16[64,2048]{1,0:T(8,128)(2,1)S(1)}, bf16[64,2048]{1,0:T(8,128)(2,1)}, u32[]{:S(2)}) copy-start(bf16[64,2048]{1,0:T(8,128)(2,1)} %get-tuple-element.5) | copy-start | bytes 786436

commit v5 on v4

--- a/solution.py
+++ b/solution.py
@@ -16,9 +16,9 @@
 
 
 def layer(
-    moe_in, moe_gain, routes, weights, taps_in, gain, shift, conv_hbm, proj_hbm, gate_hbm, up_hbm, down_hbm,
+    moe_in_hbm, moe_gain_hbm, routes_hbm, weights_hbm, taps_in_hbm, gain_hbm, shift_hbm, conv_hbm, proj_hbm, gate_hbm, up_hbm, down_hbm,
     conv_out, moe_out,
-    padded, history, taps, mixed, sums, stats, stats_in, columns, active, xin, conv_sum, wfull,
+    moe_in, moe_gain, routes, weights, taps_in, gain, shift, padded, history, taps, mixed, sums, stats, stats_in, columns, active, xin, conv_sum, wfull,
     gate, up, down, own, group, ranks, held_w, scale, outgoing, arrived, pieces,
     moe_a, moe_b, moe_c, moe_d, moe_u, moe_v, back_out, returned, running, combined, final,
     load_sem, ready, hist_send, hist_recv, a2a_send, a2a_recv,
@@ -103,12 +103,21 @@
         loads.append(pltpu.make_async_copy(gate_hbm.at[0, aligned(at, col), :], gate.at[k], load_sem.at[2]))
         loads.append(pltpu.make_async_copy(up_hbm.at[0, aligned(at, col), :], up.at[k], load_sem.at[3]))
         loads.append(pltpu.make_async_copy(down_hbm.at[0, :, aligned(at, col)], down.at[k], load_sem.at[4]))
-    for load in loads:
+    small = [
+        pltpu.make_async_copy(src, dst, load_sem.at[5 + n])
+        for n, (src, dst) in enumerate((
+            (moe_in_hbm, moe_in), (moe_gain_hbm, moe_gain), (routes_hbm, routes), (weights_hbm, weights),
+            (taps_in_hbm, taps_in), (gain_hbm, gain), (shift_hbm, shift),
+        ))
+    ]
+    for load in small + loads:
         load.start()
 
     def loaded(ref, n):
         pltpu.make_async_copy(ref, ref, load_sem.at[n]).wait()
 
+    for load in small:
+        load.wait()
     value = moe_in[...].astype(f32)
     normed = (
         value * lax.rsqrt(jnp.mean(value * value, axis=1, keepdims=True) + 1e-06) * moe_gain[...]
@@ -627,9 +636,12 @@
     hid = gate_proj.shape[2]
     chunk = xs * cs * cap
     per = xs * cs
+    reach = conv_kernel.shape[0] - 1
     vmem, dma = pltpu.VMEM, pltpu.SemaphoreType.DMA
     at_vmem, at_hbm = pl.BlockSpec(memory_space=pltpu.VMEM), pl.BlockSpec(memory_space=pltpu.HBM)
     scratch = [
+        vmem((rows, width), bf16), vmem((1, width), f32), vmem((2, group_rows), i32), vmem((2, group_rows), f32),
+        vmem((reach + 1, conv_width), bf16), vmem((1, conv_width), f32), vmem((1, conv_width), f32),
         vmem((32 + conv_rows, conv_width), bf16),
         vmem((32, conv_width), bf16),
         vmem((32, conv_width), f32),
@@ -657,7 +669,7 @@
         vmem((group_rows, col), f32),
         vmem((group_rows, col), bf16),
         vmem((4, rows, col), bf16),
-        dma((5,)), pltpu.SemaphoreType.REGULAR,
+        dma((12,)), pltpu.SemaphoreType.REGULAR,
         dma, dma,
         dma, dma,
         dma, dma((3,)),
@@ -678,7 +690,7 @@
             jax.ShapeDtypeStruct((span, width), bf16),
             jax.ShapeDtypeStruct((rows, width), bf16),
         ),
-        in_specs=[at_vmem] * 7 + [at_hbm] * 5,
+        in_specs=[at_hbm] * 12,
         out_specs=(at_vmem, at_vmem),
         scratch_shapes=scratch,
         compiler_params=pltpu.CompilerParams(

time: 114 us -> 114 us (level)
  no operation moved by 1% of the time
where the time goes in v5:
time: 114 us
  Pallas kernels  110 us (96%)
  local copies, waits for them, and re-layouts  3.05 us (3%)
    pallas_call x1, Pallas kernels, local(): pl.pallas_call(functools.partial(layer, dims=dims, cap=cap), out_shape=(j...  110 us
    unnamed x4, local copies, waits for them, and re-layouts  3.05 us

profile of v5, /device:TPU:1, one launch (start us, length us, event | category | flops | bytes accessed | tf_op | source)
XLA Modules:
  0.0 113.6 jit_solution(14236370976225342870)
XLA Ops:
  0.6 109.9 %shard_map.131 = (bf16[256,2048]{1,0:T(8,128)(2,1)}, bf16[64,2048]{1,0:T(8,128)(2,1)}) custom-call(bf16[64,2048]{1,0:T(8,128)(2,1)} %moe_in_hbm.1, f32[1,2048]{1,0:T(1,128)} %bitcast.5, s32[2,256]{1,0:T(2,128)} %bitcast.6, f32[2,256]{1,0:T(2,128)} %bitcast.7, bf16[31,512]{1,0:T(8,128)(2,1)} %taps_in_hbm.1, f32[1,512]{1,0:T(1,128)} %bitcast.8, ...), custom_call_target="tpu_custom_call" | custom-call | tf_op jit(solution)/shard_map/pallas_call | solution.py:687
  110.5 0.0 copy-start
  110.5 2.3 %copy.16 = bf16[256,2048]{1,0:T(8,128)(2,1)} copy(bf16[256,2048]{1,0:T(8,128)(2,1)} %get-tuple-element.4) | data formatting | bytes 2097152
  112.9 0.0 copy-done
  112.9 0.7 copy.17
Async XLA Ops:
  110.5 2.4 %copy-start = (bf16[64,2048]{1,0:T(8,128)(2,1)S(1)}, bf16[64,2048]{1,0:T(8,128)(2,1)}, u32[]{:S(2)}) copy-start(bf16[64,2048]{1,0:T(8,128)(2,1)} %get-tuple-element.5) | copy-start | bytes 786436
